TPU v7x, 512 devices: a whole 4x8x8 slice. The times are simulated.
512 devices in a mesh: sp: 64 (over z, y), tp: 8 (over x, core).
Axes of the slice: x: 4, y: 8, z: 8, core: 2. Of those that a mesh axis runs over, the one named last changes fastest.
Arguments:
- residual: bfloat16 [10240, 2048], P('sp'), may hold values from -6 to 6
- queries: bfloat16 [10240, 8, 128], P('sp', 'tp'), may hold values from -6 to 6
- key_vectors: bfloat16 [10240, 8, 128], P('sp', 'tp'), may hold values from -6 to 6
- value_vecs: bfloat16 [10240, 8, 128], P('sp', 'tp'), may hold values from -6 to 6
- lambda_head: float32 [8], P('tp'), may hold values from 0.3 to 0.8
- head_gain: bfloat16 [128], replicated, may hold values from 0.099609375 to 1.8984375
- w_out: bfloat16 [1024, 2048], P('tp'), may hold values from -0.1875 to 0.1875
- mlp_gain: bfloat16 [2048], replicated, may hold values from 0.099609375 to 1.8984375
- w_gate: bfloat16 [2048, 5632], P('sp', 'tp'), may hold values from -0.125 to 0.125
- w_up: bfloat16 [2048, 5632], P('sp', 'tp'), may hold values from -0.125 to 0.125
- w_down: bfloat16 [5632, 2048], P('tp', 'sp'), may hold values from -0.078125 to 0.078125
Outputs:
- layer_out: bfloat16 [10240, 2048], P(('sp', 'tp'))
All inputs are finite; a program needn't handle non-finite values.
Results may differ from a plain program's by a relative error of at most 0.014.
Values may be sent and summed in bfloat16 or wider, within the bound.
A program may use at most 128 MiB of HBM per device.

v0:
```python
import math

import jax
import jax.numpy as jnp
from jax import lax
from jax.sharding import PartitionSpec as P


def turned_gather(arrays, axis, dims):
    turned = [jnp.moveaxis(a, dim, 0) for a, dim in zip(arrays, dims)]
    both = jnp.concatenate([t.reshape(len(t), -1) for t in turned], axis=1)
    result, at, done = (lax.all_gather(both, axis, axis=0, tiled=True), 0, [])
    for t, dim in zip(turned, dims):
        section = result[:, at : at + t[0].size].reshape(-1, *t.shape[1:])
        done.append(jnp.moveaxis(section, 0, dim))
        at += t[0].size
    return tuple(done)


def side_by_side(arrays, axis, dim, along):
    both = jnp.concatenate(arrays, axis=along)
    result, at, done = (lax.all_gather(both, axis, axis=dim, tiled=True), 0, [])
    for a in arrays:
        done.append(lax.slice_in_dim(result, at, at + a.shape[along], axis=along))
        at += a.shape[along]
    return tuple(done)


def cut_along(x, dim, peers):
    shape = x.shape
    parts = x.reshape(*shape[:dim], peers, shape[dim] // peers, *shape[dim + 1 :])
    return jnp.moveaxis(parts, dim, 0)


def sent_and_summed(x, axis, dim):
    parts = cut_along(x, dim, lax.axis_size(axis))
    arrived = lax.all_to_all(parts, axis, split_axis=0, concat_axis=0, tiled=True)
    return arrived.astype(jnp.float32).sum(axis=0)


def from_everyone(x, axis):
    peers = lax.axis_size(axis)
    return lax.all_to_all(jnp.broadcast_to(x[None], (peers, *x.shape)), axis, 0, 0, tiled=True)


def in_order(parts, dim):
    parts = jnp.moveaxis(parts, 0, dim)
    shape = parts.shape
    return parts.reshape(*shape[:dim], shape[dim] * shape[dim + 1], *shape[dim + 2 :])


def gather_directly(x, axis, dim):
    parts = from_everyone(x, axis)
    return in_order(parts, dim)


def rms_rows(matrix, gain_vec):
    floats = matrix.astype(jnp.float32)
    scaled = floats * lax.rsqrt(jnp.mean(floats * floats, axis=-1, keepdims=True) + 1e-06)
    return (scaled * gain_vec.astype(jnp.float32)).astype(jnp.bfloat16)


def keep_state(current):
    return current


def local(
    residual,
    queries,
    key_vectors,
    value_vecs,
    lambda_head,
    head_gain,
    w_out,
    mlp_gain,
    w_gate,
    w_up,
    w_down,
):
    tok_rows = queries.shape[0]
    heads_here = queries.shape[1]
    key_width = queries.shape[2] // 2
    head_width = value_vecs.shape[2]
    row_share = tok_rows // lax.axis_size("tp")
    own_start = lax.axis_index("tp") * row_share
    full_gate, full_up, full_down = turned_gather((w_gate, w_up, w_down), "sp", (0, 0, 1))
    first_row = lax.axis_index("sp") * tok_rows
    last_row = first_row + tok_rows - 1
    query_pos = first_row + jnp.arange(tok_rows, dtype=jnp.int32)
    score_scale = 1.0 / math.sqrt(key_width)
    initial = (
        jnp.full((2, heads_here, tok_rows), -jnp.inf, jnp.float32),
        jnp.zeros((2, heads_here, tok_rows), jnp.float32),
        jnp.zeros((2, heads_here, tok_rows, head_width), jnp.float32),
    )
    piece_keys, piece_values = side_by_side((key_vectors, value_vecs), "sp", 0, 1)
    piece_len = piece_keys.shape[0]

    def update(current):
        maxima, totals, acc_sum = current
        key_pos = jnp.arange(piece_len, dtype=jnp.int32)
        causal = key_pos[None, :] <= query_pos[:, None]
        new_max, new_tot, new_acc = ([], [], [])
        for member in range(2):
            lower_col = member * key_width
            scores = (
                jnp.einsum(
                    "qhd,khd->hqk",
                    queries[:, :, lower_col : lower_col + key_width],
                    piece_keys[:, :, lower_col : lower_col + key_width],
                    preferred_element_type=jnp.float32,
                )
                * score_scale
            )
            scores = jnp.where(causal[None], scores, -jnp.inf)
            peak_score = jnp.max(scores, axis=-1)
            safe_peak = jnp.where(peak_score == -jnp.inf, 0.0, peak_score)
            weights = jnp.exp(scores - safe_peak[..., None])
            rescale = jnp.exp(maxima[member] - safe_peak)
            new_tot.append(totals[member] * rescale + jnp.sum(weights, axis=-1))
            new_acc.append(
                acc_sum[member] * rescale[..., None]
                + jnp.einsum(
                    "hqk,khe->hqe",
                    weights.astype(jnp.bfloat16),
                    piece_values,
                    preferred_element_type=jnp.float32,
                )
            )
            new_max.append(peak_score)
        return (jnp.stack(new_max), jnp.stack(new_tot), jnp.stack(new_acc))

    maxima, totals, acc_sum = lax.cond(jnp.int32(0) <= last_row, update, keep_state, initial)
    read_out = acc_sum / totals[..., None]
    difference = read_out[0] - lambda_head[:, None, None] * read_out[1]
    heads_out = rms_rows(difference, head_gain)
    heads_flat = jnp.transpose(heads_out, (1, 0, 2)).reshape(tok_rows, heads_here * head_width)
    picked = heads_flat
    projected = sent_and_summed(
        jnp.dot(picked, w_out, preferred_element_type=jnp.float32).astype(jnp.bfloat16), "tp", 0
    )
    own_resid = lax.dynamic_slice_in_dim(residual, own_start, row_share, 0)
    middle = (own_resid.astype(jnp.float32) + projected).astype(jnp.bfloat16)
    normed = gather_directly(rms_rows(middle, mlp_gain), "tp", 0)
    gate_act = jnp.dot(normed, full_gate, preferred_element_type=jnp.float32)
    up_act = jnp.dot(normed, full_up, preferred_element_type=jnp.float32)
    hidden = (jax.nn.silu(gate_act) * up_act).astype(jnp.bfloat16)
    picked = hidden
    down_sum = sent_and_summed(
        jnp.dot(picked, full_down, preferred_element_type=jnp.float32).astype(jnp.bfloat16), "tp", 0
    )
    return (middle.astype(jnp.float32) + 0.5 * down_sum).astype(jnp.bfloat16)


def solution(mesh):
    in_specs = (
        P("sp", None),
        P("sp", "tp", None),
        P("sp", "tp", None),
        P("sp", "tp", None),
        P("tp"),
        P(),
        P("tp", None),
        P(),
        P("sp", "tp"),
        P("sp", "tp"),
        P("tp", "sp"),
    )
    out_specs = P(("sp", "tp"), None)
    return jax.shard_map(local, mesh=mesh, in_specs=in_specs, out_specs=out_specs, check_vma=False)
```

profile of v0, /device:TPU:1, one launch (start us, length us, event | category | flops | bytes accessed | tf_op | source)
XLA Modules:
  0.0 237.4 jit_solution(10475612362510131676)
XLA Ops:
  6.5 0.0 copy-start
  6.5 0.0 all-gather.3.cloned.1.call-start
  6.5 0.9 copy.21
  7.4 0.8 copy.22
  8.3 0.8 pad_maximum_fusion.2
  9.1 0.0 all-gather.3.cloned.1.call-update
  9.1 0.0 all-gather.5.cloned.1.call-start
  9.2 1.6 concatenate.7
  10.8 0.0 all-gather.5.cloned.1.call-update
  11.5 0.7 convert_element_type.56
  12.1 87.9 %all-gather.3.cloned.1.call-done = bf16[10240,2,128]{2,1,0:T(2,128)(2,1)} async-done(((bf16[160,2,128]{2,1,0:T(2,128)(2,1)}), bf16[10240,2,128]{2,1,0:T(2,128)(2,1)}) %all-gather.3.cloned.1.call-update) | async-done | bytes 5242896 | tf_op jit(solution)/shard_map/all_gather | solution.py:22
  100.0 0.0 copy-start.2
  100.0 29.9 %conditional.1 = (f32[2,1,160]{2,1,0:T(1,128)S(1)}, f32[2,1,160,128]{3,2,1,0:T(8,128)S(1)}) conditional(s32[]{:T(128)} %convert_element_type.55, () %tuple.13, (s32[]{:T(128)}, s32[160]{0:T(256)S(1)}, bf16[160,1,128]{2,0,1:T(8,128)(2,1)}, bf16[10240,2,128]{2,1,0:T(2,128)(2,1)}) %tuple.14), branch_computations={%region_0.0_spmd, %region_1.6_spmd} | conditional | flops 1284590208 | bytes 89789488 | solution.py:133
  100.0 0.9 copy.23
  100.9 4.7 %copy.20 = bf16[10240,2,128]{2,0,1:T(8,128)(2,1)} copy(bf16[10240,2,128]{2,1,0:T(2,128)(2,1)} %get-tuple-element.39) | data formatting | bytes 10485760 | tf_op jit(solution)/shard_map
  105.6 13.8 %copy.24 = bf16[10240,2,128]{0,2,1:T(8,128)(2,1)} copy(bf16[10240,2,128]{2,1,0:T(2,128)(2,1)} %get-tuple-element.39) | data formatting | bytes 10485760 | tf_op jit(solution)/shard_map
  119.4 0.0 copy-start.1
  119.4 2.9 %fusion.68 = (f32[160]{0:T(256)S(1)}, f32[160,10240]{1,0:T(8,128)S(1)}) fusion(bf16[10240,2,128]{0,2,1:T(8,128)(2,1)} %copy.24, bf16[160,1,128]{0,2,1:T(8,128)(2,1)S(1)} %copy.23, s32[160]{0:T(256)S(1)} %broadcast_add_fusion), kind=kOutput, calls=%fused_computation.82 | convolution fusion | flops 216268640 | bytes 7898752 | tf_op jit(solution)/shard_map/cond/branch_1_fun/qhd,khd->hqk/dot_general | solution.py:107
  122.3 1.1 fusion.3
  123.4 0.0 copy-done.1
  123.4 1.3 fusion.15
  124.7 2.8 %fusion.67 = (f32[160]{0:T(256)S(1)}, f32[160,10240]{1,0:T(8,128)S(1)}) fusion(bf16[10240,2,128]{0,2,1:T(8,128)(2,1)} %copy.24, bf16[160,1,128]{0,2,1:T(8,128)(2,1)S(1)} %copy.23, s32[160]{0:T(256)S(1)} %broadcast_add_fusion), kind=kOutput, calls=%fused_computation.81 | convolution fusion | flops 216268640 | bytes 7898752 | tf_op jit(solution)/shard_map/cond/branch_1_fun/qhd,khd->hqk/dot_general | solution.py:107
  127.5 1.3 fusion.21
  128.8 1.1 fusion.5
  130.0 0.1 broadcast_divide_fusion
  130.1 0.1 multiply_reduce_fusion
  130.2 0.0 copy-done
  130.2 0.4 convolution_convert_fusion
  130.6 1.1 reshape.249
  131.7 8.8 %all-to-all-start = ((bf16[8,20,2048]{2,1,0:T(8,128)(2,1)}), bf16[8,20,2048]{2,1,0:T(8,128)(2,1)S(1)}, u32[]{:S(2)}, u32[]{:S(2)}) async-start(bf16[8,20,2048]{2,1,0:T(8,128)(2,1)} %reshape.249), calls=%async_computation | async-start | bytes 1572864 | tf_op jit(solution)/shard_map/all_to_all | solution.py:37
  140.5 0.0 copy-done.2
  140.5 12.2 %all-to-all-done = bf16[8,20,2048]{2,1,0:T(8,128)(2,1)S(1)} async-done(((bf16[8,20,2048]{2,1,0:T(8,128)(2,1)}), bf16[8,20,2048]{2,1,0:T(8,128)(2,1)S(1)}, u32[]{:S(2)}, u32[]{:S(2)}) %all-to-all-start) | async-done | bytes 655392 | tf_op jit(solution)/shard_map/all_to_all | solution.py:37
  152.7 0.1 convert_reduce_fusion.1
  152.8 1.1 fusion.55
  153.9 0.1 fusion.57
  154.0 0.1 broadcast_in_dim.28
  154.1 15.6 %all_to_all.15 = bf16[8,20,2048]{2,1,0:T(8,128)(2,1)S(1)} all-to-all(bf16[8,20,2048]{2,1,0:T(8,128)(2,1)S(1)} %broadcast_in_dim.28), channel_id=1, replica_groups=mesh['sp'=64,'tp'=8] {'tp'}, dimensions={0} | all-to-all | bytes 1310720 | tf_op jit(solution)/shard_map/all_to_all | solution.py:43
  169.7 0.1 reshape.250
  169.8 34.9 %all-gather.5.cloned.1.call-done = bf16[2048,2112]{1,0:T(8,128)(2,1)} async-done(((bf16[32,2112]{1,0:T(8,128)(2,1)}), bf16[2048,2112]{1,0:T(8,128)(2,1)}) %all-gather.5.cloned.1.call-update) | async-done | bytes 8650768 | tf_op jit(solution)/shard_map/all_gather | solution.py:12
  204.7 2.6 %fusion.36 = f32[160,704]{1,0:T(8,128)S(1)} fusion(bf16[160,2048]{1,0:T(8,128)(2,1)S(1)} %reshape.250, bf16[2048,2112]{1,0:T(8,128)(2,1)} %all-gather.5.cloned.1.call-done), kind=kOutput, calls=%fused_computation.45 | convolution fusion | flops 461373440 | bytes 4251648 | tf_op jit(solution)/shard_map/dot_general | solution.py:145
  207.3 5.3 %fusion.38 = bf16[160,2048]{1,0:T(8,128)(2,1)S(1)} fusion(bf16[2048,2112]{1,0:T(8,128)(2,1)} %all-gather.5.cloned.1.call-done, bf16[160,2048]{1,0:T(8,128)(2,1)S(1)} %reshape.250, f32[160,704]{1,0:T(8,128)S(1)} %fusion.36), kind=kOutput, calls=%fused_computation.47 | convolution fusion | flops 923750400 | bytes 8052736 | tf_op jit(solution)/shard_map/dot_general | solution.py:150
  212.6 0.1 reshape.251
  212.7 17.0 %all_to_all.16 = bf16[8,20,2048]{2,1,0:T(8,128)(2,1)S(1)} all-to-all(bf16[8,20,2048]{2,1,0:T(8,128)(2,1)S(1)} %reshape.251), channel_id=1, replica_groups=mesh['sp'=64,'tp'=8] {'tp'}, dimensions={0} | all-to-all | bytes 1310720 | tf_op jit(solution)/shard_map/all_to_all | solution.py:37
  229.7 0.1 convert_reduce_fusion
  229.9 0.7 fusion.58
  (11 shorter events, 0.1 us)
Async XLA Ops:
  6.5 123.7 %copy-start = (bf16[128,2048]{1,0:T(8,128)(2,1)S(1)}, bf16[128,2048]{1,0:T(8,128)(2,1)}, u32[]{:S(2)}) copy-start(bf16[128,2048]{1,0:T(8,128)(2,1)} %param.19) | copy-start | bytes 1572868
  6.5 93.5 %all-gather.3.cloned.1.call-start = ((), (), s32[]{:S(2)}) async-start(), calls=%async_computation.3 | async-start | bytes 5324800 | tf_op jit(solution)/shard_map/all_gather | solution.py:22
  9.1 195.6 %all-gather.5.cloned.1.call-start = ((), (), s32[]{:S(2)}) async-start(), calls=%async_computation.4 | async-start | bytes 9052160 | tf_op jit(solution)/shard_map/all_gather | solution.py:12
  100.0 40.5 %copy-start.2 = (bf16[2048]{0:T(1024)(128)(2,1)S(1)}, bf16[2048]{0:T(1024)(128)(2,1)}, u32[]{:S(2)}) copy-start(bf16[2048]{0:T(1024)(128)(2,1)} %param.20) | copy-start | bytes 12292
  119.4 4.1 %copy-start.1 = (bf16[10240,2,128]{2,0,1:T(8,128)(2,1)S(1)}, bf16[10240,2,128]{2,0,1:T(8,128)(2,1)}, u32[]{:S(2)}) copy-start(bf16[10240,2,128]{2,0,1:T(8,128)(2,1)} %copy.20) | copy-start | bytes 15728644 | tf_op jit(solution)/shard_map/cond
  131.7 21.0 %all-to-all-start = ((bf16[8,20,2048]{2,1,0:T(8,128)(2,1)}), bf16[8,20,2048]{2,1,0:T(8,128)(2,1)S(1)}, u32[]{:S(2)}, u32[]{:S(2)}) async-start(bf16[8,20,2048]{2,1,0:T(8,128)(2,1)} %reshape.249), calls=%async_computation | async-start | bytes 1572864 | tf_op jit(solution)/shard_map/all_to_all | solution.py:37
Sparse Core Ops, SparseCore 0:
  10.3 89.6 all-gather.2
  103.0 101.6 all-gather.4
where the time goes:
time: 238 us; the launch traced here: 237 us
  waiting for transfers between devices  135 us (57%)
  blocking collectives  32.6 us (14%)
  local copies, waits for them, and re-layouts  24.1 us (10%)
  matrix products  16.4 us (7%)
  between operations  14.2 us (6%)
  starting transfers between devices  8.88 us (4%)
  other arithmetic  6.14 us (3%)
    all_gather x1, waiting for transfers between devices, side_by_side(): result, at, done = (lax.all_gather(both, axis, axis=dim, tiled=True), 0, [])  87.9 us
    all_gather x1, waiting for transfers between devices, turned_gather(): result, at, done = (lax.all_gather(both, axis, axis=0, tiled=True), 0, [])  34.9 us
    another operation x3, local copies, waits for them, and re-layouts  19.3 us
    all_to_all x1, blocking collectives, sent_and_summed(): lax.all_to_all(parts, axis, split_axis=0, concat_axis=0, tiled=True)  17 us
    all_to_all x1, blocking collectives, from_everyone(): lax.all_to_all(jnp.broadcast_to(x[None], (peers, *x.shape)), axis, 0, 0,...  15.6 us
    all_to_all x1, waiting for transfers between devices, sent_and_summed(): lax.all_to_all(parts, axis, split_axis=0, concat_axis=0, tiled=True)  12.2 us
    all_to_all x1, starting transfers between devices, sent_and_summed(): lax.all_to_all(parts, axis, split_axis=0, concat_axis=0, tiled=True)  8.84 us
    dot_general x2, matrix products, update(): jnp.einsum('qhd,khd->hqk', queries[:, :, lower_col:lower_col + key_width]...  5.7 us
  transfers between devices with their start and end apart: 3, of which 3 were waited for; matrix products, arithmetic and copies ran while one was open for 15% of the time, Pallas kernels for 0%

commit v1 on v0

v1 whole, which is shorter than its diff:
```python
import functools

import jax
import jax.numpy as jnp
from jax import lax
from jax.experimental import pallas as pl
from jax.experimental.pallas import tpu as pltpu
from jax.sharding import PartitionSpec as P

MESH = pl.DeviceIdType.MESH
RING = 8
ROWS = 160
SHARE = 20
WIDTH = 128
MODEL = 2048
GATED = 1408
PACKED = 2176
FAR = -1e30
DIRS = (1, -1)
HALF_STEPS = {1: 4, -1: 3}


def wrap(v):
    return lax.rem(v + 2 * RING, RING)


def nt_dot(a, b, precision=None):
    return lax.dot_general(
        a, b, (((1,), (1,)), ((), ())), preferred_element_type=jnp.float32, precision=precision
    )


def layer(
    lam_ref, resid_hbm, q_ref, k_ref, v_ref, hgain_ref, wo_hbm, mgain_ref, shard_hbm, out_ref,
    weights, wo_all, qg, kg, vext, o_send, o_recv, st_send, st_recv, heads_out, heads_all,
    resid, mid, normed, hidden, piece, own_mid, d_send, d_recv,
    ring1_send, ring1_recv, ring2_send, ring2_recv, q_ss, q_rs, k_ss, k_rs, v_ss, v_rs,
    o_ss, o_rs, st_ss, st_rs, wo_ss, wo_rs, core_ss, core_rs, h_ss, h_rs, d_ss, d_rs, local_sem,
):
    sp = lax.axis_index("sp")
    tp = lax.axis_index("tp")
    z = lax.div(sp, RING)
    y = lax.rem(sp, RING)

    def at_zy(zz, yy):
        return {"sp": zz * RING + yy}

    def remote(src, dst, ss, rs, device):
        return pltpu.make_async_remote_copy(
            src_ref=src, dst_ref=dst, send_sem=ss, recv_sem=rs, device_id=device, device_id_type=MESH
        )

    qg[y] = q_ref[...]
    kg[z] = k_ref[...]
    vext[z, :, 0:WIDTH] = v_ref[...]
    vext[:, :, WIDTH : 2 * WIDTH] = jnp.ones((RING, ROWS, WIDTH), jnp.bfloat16)

    barrier = pltpu.get_barrier_semaphore()
    for j in range(1, RING):
        pl.semaphore_signal(barrier, inc=1, device_id=at_zy(z, wrap(y + j)), device_id_type=MESH)
        pl.semaphore_signal(barrier, inc=1, device_id=at_zy(wrap(z + j), y), device_id_type=MESH)
        pl.semaphore_signal(barrier, inc=1, device_id={"tp": wrap(tp + j)}, device_id_type=MESH)

    local_shard = [
        pltpu.make_async_copy(shard_hbm.at[h], weights.at[z, y, h], local_sem.at[h]) for h in range(2)
    ]
    local_resid = pltpu.make_async_copy(resid_hbm, resid, local_sem.at[2])
    local_wo = pltpu.make_async_copy(wo_hbm, wo_all.at[tp], local_sem.at[3])
    for c in local_shard + [local_resid, local_wo]:
        c.start()
    pl.semaphore_wait(barrier, 3 * (RING - 1))

    def q_copy(j, src_slot):
        return remote(q_ref, qg.at[src_slot], q_ss.at[j], q_rs.at[j], at_zy(z, wrap(y + j + 1)))

    def k_copy(j, src_slot):
        return remote(k_ref, kg.at[src_slot], k_ss.at[j], k_rs.at[j], at_zy(wrap(z + j + 1), y))

    def v_copy(j, src_slot):
        return remote(
            v_ref, vext.at[src_slot, :, pl.ds(0, WIDTH)], v_ss.at[j], v_rs.at[j], at_zy(wrap(z + j + 1), y)
        )

    for j in (0, 6, 1, 5, 2, 4, 3):
        k_copy(j, z).start()
        v_copy(j, z).start()
        q_copy(j, y).start()

    def ring1(h, d, k, arriving=False):
        back = k if arriving else k - 1
        if h == 0:
            slot = weights.at[z, wrap(y - d * back), 0]
            device = at_zy(z, wrap(y + d))
        else:
            slot = weights.at[wrap(z - d * back), y, 1]
            device = at_zy(wrap(z + d), y)
        index = (h * 2 + (d < 0)) * 4 + k - 1
        src = shard_hbm.at[h] if (k == 1 and not arriving) else slot
        return remote(src, slot, ring1_send.at[index], ring1_recv.at[index], device)

    def ring2_steps(d, sub):
        return HALF_STEPS[d] if sub == 0 else HALF_STEPS[-d]

    def ring2(h, d, sub, k, arriving=False):
        back = k if arriving else k - 1
        if h == 0:
            slot = weights.at[wrap(z - d * back), pl.ds(4 * sub, 4), 0]
            device = at_zy(wrap(z + d), y)
        else:
            slot = weights.at[pl.ds(4 * sub, 4), wrap(y - d * back), 1]
            device = at_zy(z, wrap(y + d))
        index = ((h * 2 + (d < 0)) * 2 + sub) * 4 + k - 1
        return remote(slot, slot, ring2_send.at[index], ring2_recv.at[index], device)

    def wo_copy(j, slot):
        return remote(wo_hbm, wo_all.at[slot], wo_ss.at[j], wo_rs.at[j], {"tp": wrap(tp + 2 * (j + 1))})

    partner = tp + 1 - 2 * lax.rem(tp, 2)

    def core_copy(j, slot):
        return remote(wo_all.at[slot], wo_all.at[slot], core_ss.at[j], core_rs.at[j], {"tp": partner})

    for h in range(2):
        for d in DIRS:
            ring1(h, d, 1).start()
    for j in (0, 2, 1):
        wo_copy(j, tp).start()

    for k in range(1, 5):
        for d in DIRS:
            for h in range(2):
                if k <= HALF_STEPS[d]:
                    ring1(h, d, k, True).wait_recv()
                    if k < HALF_STEPS[d]:
                        ring1(h, d, k + 1).start()
    for c in local_shard:
        c.wait()

    for sub in range(2):
        for h in range(2):
            for d in DIRS:
                ring2(h, d, sub, 1).start()

    def ring2_forward(sub, k):
        for h in range(2):
            for d in DIRS:
                if k <= ring2_steps(d, sub):
                    ring2(h, d, sub, k, True).wait_recv()
                    if k < ring2_steps(d, sub):
                        ring2(h, d, sub, k + 1).start()

    for j in range(7):
        q_copy(j, wrap(y - j - 1)).wait_recv()
        k_copy(j, wrap(z - j - 1)).wait_recv()
        v_copy(j, wrap(z - j - 1)).wait_recv()

    lane = lax.broadcasted_iota(jnp.int32, (ROWS, WIDTH), 1)
    key_lane = lax.broadcasted_iota(jnp.int32, (1, RING * ROWS), 1)
    key_pos = key_lane + y * ROWS
    for j in range(1, RING):
        key_pos = key_pos + jnp.where(key_lane >= j * ROWS, (RING - 1) * ROWS, 0)
    row_iota = lax.broadcasted_iota(jnp.int32, (ROWS, 1), 0)
    pick = (
        lax.broadcasted_iota(jnp.int32, (8, WIDTH), 1) == 64 * lax.broadcasted_iota(jnp.int32, (8, WIDTH), 0)
    ).astype(jnp.float32)
    spread = (
        lax.div(lax.broadcasted_iota(jnp.int32, (8, 2 * WIDTH), 1), WIDTH)
        == lax.broadcasted_iota(jnp.int32, (8, 2 * WIDTH), 0)
    ).astype(jnp.float32)

    def o_copy(i, src_slot):
        return remote(o_send.at[i], o_recv.at[src_slot], o_ss.at[i], o_rs.at[i], at_zy(z, wrap(y + i + 1)))

    def st_copy(i, src_slot):
        return remote(st_send.at[i], st_recv.at[src_slot], st_ss.at[i], st_rs.at[i], at_zy(z, wrap(y + i + 1)))

    def attend(i, own):
        yq = y if own else wrap(y + i + 1)
        q = qg[yq] * jnp.bfloat16(0.125)
        q_pos = z * (RING * ROWS) + yq * ROWS + row_iota
        seen = key_pos <= q_pos
        keys = kg[...].reshape(RING * ROWS, WIDTH)
        vals = vext[...].reshape(RING * ROWS, 2 * WIDTH)
        logs = []
        for m in range(2):
            half = (lane < 64) if m == 0 else (lane >= 64)
            qm = jnp.where(half, q.astype(jnp.float32), 0.0).astype(jnp.bfloat16)
            s = jnp.where(seen, nt_dot(qm, keys), FAR)
            top = jnp.max(s, axis=1, keepdims=True)
            p = jnp.exp(s - top).astype(jnp.bfloat16)
            both = jnp.dot(p, vals, preferred_element_type=jnp.float32)
            total = both[:, WIDTH:]
            reading = (both[:, :WIDTH] / total).astype(jnp.bfloat16)
            if own:
                o_recv[y, m] = reading
            else:
                o_send[i, m] = reading
            logs.append(top + jnp.log(total))
        stats = nt_dot(pick, jnp.where(lane < 64, logs[0], logs[1]), lax.Precision.HIGHEST)
        if own:
            st_recv[y] = stats
        else:
            st_send[i] = stats
            o_copy(i, y).start()
            st_copy(i, y).start()

    def attend_step(i, carry):
        attend(i, False)
        return carry

    lax.fori_loop(0, 4, attend_step, 0)
    ring2_forward(0, 1)
    lax.fori_loop(4, 7, attend_step, 0)
    attend(7, True)
    ring2_forward(1, 1)

    local_wo.wait()
    for j in range(3):
        wo_copy(j, wrap(tp - 2 * (j + 1))).wait_recv()
    for j in range(4):
        core_copy(j, wrap(tp + 2 * j)).start()

    for i in range(7):
        o_copy(i, wrap(y - i - 1)).wait_recv()
        st_copy(i, wrap(y - i - 1)).wait_recv()

    stat = [lax.dot_general(st_recv[p], spread, (((0,), (0,)), ((), ())), preferred_element_type=jnp.float32,
                            precision=lax.Precision.HIGHEST) for p in range(RING)]
    readings = []
    for m in range(2):
        ls = [s[:, m * WIDTH : (m + 1) * WIDTH] for s in stat]
        top = functools.reduce(jnp.maximum, ls)
        share = [jnp.exp(l - top) for l in ls]
        total = functools.reduce(jnp.add, share)
        acc = functools.reduce(jnp.add, [share[p] * o_recv[p, m].astype(jnp.float32) for p in range(RING)])
        readings.append(acc / total)
    diff = readings[0] - lam_ref[0] * readings[1]
    scale = lax.rsqrt(jnp.mean(diff * diff, axis=1, keepdims=True) + 1e-06)
    heads = (diff * scale * hgain_ref[...].astype(jnp.float32)).astype(jnp.bfloat16)
    heads_out[...] = heads

    def h_copy(j, slot):
        lanes = pl.ds(pl.multiple_of(slot * WIDTH, WIDTH), WIDTH)
        return remote(heads_out, heads_all.at[:, lanes], h_ss.at[j], h_rs.at[j], {"tp": wrap(tp + j + 1)})

    for j in range(7):
        h_copy(j, tp).start()
    heads_all[:, pl.ds(pl.multiple_of(tp * WIDTH, WIDTH), WIDTH)] = heads
    ring2_forward(0, 2)
    local_resid.wait()
    for j in range(4):
        core_copy(j, wrap(partner + 2 * j)).wait_recv()
    for j in range(7):
        h_copy(j, wrap(tp - j - 1)).wait_recv()

    def project(c, squares):
        lanes = pl.ds(pl.multiple_of(c * 256, 256), 256)
        w = wo_all[:, :, lanes].reshape(RING * WIDTH, 256)
        part = jnp.dot(heads_all[...], w, preferred_element_type=jnp.float32)
        m = (resid[:, lanes].astype(jnp.float32) + part).astype(jnp.bfloat16).astype(jnp.float32)
        mid[:, lanes] = m
        return squares + m[:, :WIDTH] * m[:, :WIDTH] + m[:, WIDTH:] * m[:, WIDTH:]

    squares = lax.fori_loop(0, 8, project, jnp.zeros((ROWS, WIDTH), jnp.float32))
    scale = lax.rsqrt(jnp.sum(squares, axis=1, keepdims=True) * (1.0 / MODEL) + 1e-06)

    def norm(c, carry):
        lanes = pl.ds(pl.multiple_of(c * 256, 256), 256)
        normed[:, lanes] = (mid[:, lanes] * scale * mgain_ref[:, lanes].astype(jnp.float32)).astype(jnp.bfloat16)
        return carry

    lax.fori_loop(0, 8, norm, 0)
    for t in range(RING):
        @pl.when(tp == t)
        def _():
            own_mid[...] = mid[t * SHARE : (t + 1) * SHARE, :]

    ring2_forward(1, 2)
    ring2_forward(0, 3)
    ring2_forward(1, 3)
    ring2_forward(0, 4)
    ring2_forward(1, 4)

    def silu_times(g, u):
        return (g / (1.0 + jnp.exp(-g)) * u).astype(jnp.bfloat16)

    def gate_up(c, carry):
        lanes = pl.ds(pl.multiple_of(c * 256, 256), 256)
        w = weights[:, :, :, :, lanes].reshape(MODEL, 256)
        r = jnp.dot(normed[...], w, preferred_element_type=jnp.float32)
        hidden[:, pl.ds(pl.multiple_of(c * WIDTH, WIDTH), WIDTH)] = silu_times(r[:, :WIDTH], r[:, WIDTH:])
        return carry

    lax.fori_loop(0, 5, gate_up, 0)
    w = weights[:, :, :, :, GATED - WIDTH : GATED].reshape(MODEL, WIDTH)
    r = jnp.dot(normed[...], w, preferred_element_type=jnp.float32)
    r = jnp.where(lane < 64, silu_times(r, pltpu.roll(r, 64, 1)).astype(jnp.float32), 0.0)
    hidden[:, 5 * WIDTH :] = r.astype(jnp.bfloat16)

    def d_copy(j, part, dst_slot, device):
        lanes = pl.ds(part * (MODEL // 2), MODEL // 2)
        peer = wrap(tp + j + 1)
        index = part * 7 + j
        return remote(d_send.at[peer, :, lanes], d_recv.at[dst_slot, :, lanes], d_ss.at[index], d_rs.at[index],
                      {"tp": peer})

    def down(c, carry):
        w = weights[c, :, :, :, GATED:PACKED].reshape(256, PACKED - GATED)
        lanes = pl.ds(pl.multiple_of(c * 256, 256), 256)
        piece[...] = nt_dot(hidden[...], w)
        for t in range(RING):
            d_send[t, :, lanes] = piece[t * SHARE : (t + 1) * SHARE, :].astype(jnp.bfloat16)
        return carry

    for part in range(2):
        lax.fori_loop(4 * part, 4 * part + 4, down, 0)
        for j in range(7):
            d_copy(j, part, tp, None).start()

    d_recv[tp] = d_send[tp]
    for part in range(2):
        for j in range(7):
            d_copy(j, part, wrap(tp - j - 1), None).wait_recv()
    total = functools.reduce(jnp.add, [d_recv[t].astype(jnp.float32) for t in range(RING)])
    out_ref[...] = (own_mid[...] + 0.5 * total).astype(jnp.bfloat16)

    for j in range(7):
        q_copy(j, y).wait_send()
        k_copy(j, z).wait_send()
        v_copy(j, z).wait_send()
        o_copy(j, y).wait_send()
        st_copy(j, y).wait_send()
        h_copy(j, tp).wait_send()
        for part in range(2):
            d_copy(j, part, tp, None).wait_send()
    for j in range(3):
        wo_copy(j, tp).wait_send()
    for j in range(4):
        core_copy(j, wrap(tp + 2 * j)).wait_send()
    for h in range(2):
        for d in DIRS:
            for k in range(1, HALF_STEPS[d] + 1):
                ring1(h, d, k).wait_send()
            for sub in range(2):
                for k in range(1, ring2_steps(d, sub) + 1):
                    ring2(h, d, sub, k).wait_send()


def local(residual, queries, key_vectors, value_vecs, lambda_head, head_gain, w_out, mlp_gain, w_gate, w_up, w_down):
    depth = w_gate.shape[0]
    main = jnp.stack(
        [w_gate[:, :640].reshape(depth, 5, WIDTH), w_up[:, :640].reshape(depth, 5, WIDTH)], axis=2
    ).reshape(depth, 1280)
    packed = jnp.concatenate(
        [main, w_gate[:, 640:], w_up[:, 640:], w_down.T, jnp.zeros((depth, 64), jnp.bfloat16)], axis=1
    ).reshape(2, depth // 2, PACKED)
    vmem = pl.BlockSpec(memory_space=pltpu.VMEM)
    hbm = pl.BlockSpec(memory_space=pl.ANY)
    dma = pltpu.SemaphoreType.DMA
    bf, f32 = jnp.bfloat16, jnp.float32
    return pl.pallas_call(
        layer,
        out_shape=jax.ShapeDtypeStruct((SHARE, MODEL), bf),
        in_specs=[pl.BlockSpec(memory_space=pltpu.SMEM), hbm, vmem, vmem, vmem, vmem, hbm, vmem, hbm],
        out_specs=vmem,
        scratch_shapes=[
            pltpu.VMEM((RING, RING, 2, 16, PACKED), bf),
            pltpu.VMEM((RING, WIDTH, MODEL), bf),
            pltpu.VMEM((RING, ROWS, WIDTH), bf),
            pltpu.VMEM((RING, ROWS, WIDTH), bf),
            pltpu.VMEM((RING, ROWS, 2 * WIDTH), bf),
            pltpu.VMEM((RING - 1, 2, ROWS, WIDTH), bf),
            pltpu.VMEM((RING, 2, ROWS, WIDTH), bf),
            pltpu.VMEM((RING - 1, 8, ROWS), f32),
            pltpu.VMEM((RING, 8, ROWS), f32),
            pltpu.VMEM((ROWS, WIDTH), bf),
            pltpu.VMEM((ROWS, RING * WIDTH), bf),
            pltpu.VMEM((ROWS, MODEL), bf),
            pltpu.VMEM((ROWS, MODEL), f32),
            pltpu.VMEM((ROWS, MODEL), bf),
            pltpu.VMEM((ROWS, PACKED - GATED), bf),
            pltpu.VMEM((ROWS, 256), f32),
            pltpu.VMEM((SHARE, MODEL), f32),
            pltpu.VMEM((RING, SHARE, MODEL), bf),
            pltpu.VMEM((RING, SHARE, MODEL), bf),
            dma((16,)), dma((16,)), dma((32,)), dma((32,)),
            dma((7,)), dma((7,)), dma((7,)), dma((7,)), dma((7,)), dma((7,)),
            dma((7,)), dma((7,)), dma((7,)), dma((7,)),
            dma((3,)), dma((3,)), dma((4,)), dma((4,)), dma((7,)), dma((7,)), dma((14,)), dma((14,)), dma((4,)),
        ],
        compiler_params=pltpu.CompilerParams(
            collective_id=0, has_side_effects=True, vmem_limit_bytes=56 * 1024 * 1024
        ),
    )(
        lambda_head, residual, queries.reshape(ROWS, WIDTH), key_vectors.reshape(ROWS, WIDTH),
        value_vecs.reshape(ROWS, WIDTH), head_gain.reshape(1, WIDTH), w_out, mlp_gain.reshape(1, MODEL), packed,
    )


def solution(mesh):
    in_specs = (
        P("sp", None), P("sp", "tp", None), P("sp", "tp", None), P("sp", "tp", None), P("tp"), P(),
        P("tp", None), P(), P("sp", "tp"), P("sp", "tp"), P("tp", "sp"),
    )
    return jax.shard_map(
        local, mesh=mesh, in_specs=in_specs, out_specs=P(("sp", "tp"), None), check_vma=False
    )
```

time: 238 us -> 129 us (0.54)
  waiting for transfers between devices: 135 us -> 0 us
  Pallas kernels: 0 us -> 122 us
  blocking collectives: 32.6 us -> 0 us
  local copies, waits for them, and re-layouts: 24.1 us -> 5.43 us
  matrix products: 16.4 us -> 0 us
  between operations: 14.2 us -> 0.73 us
  starting transfers between devices: 8.88 us -> 0 us
  other arithmetic: 6.14 us -> 0.03 us
    all_gather x2 -> x0, waiting for transfers between devices: 123 us -> none  [the longest x1 87.9 us: side_by_side(): result, at, done = (lax.all_gather(both, axis, axis=dim, tiled=True), 0, [])]
    pallas_call x0 -> x1, Pallas kernels: none -> 122 us  [local(): pl.pallas_call(layer, out_shape=jax.ShapeDtypeStruct((SHARE, MODEL), bf),...]
    all_to_all x2 -> x0, blocking collectives: 32.6 us -> none  [the longest x1 17 us: sent_and_summed(): lax.all_to_all(parts, axis, split_axis=0, concat_axis=0, tiled=True)]
    another operation x3, local copies, waits for them, and re-layouts: 19.3 us -> 0.23 us  [local(): jnp.stack([w_gate[:, :640].reshape(depth, 5, WIDTH), w_up[:, :640].reshap...]
    dot_general x7 -> x0, matrix products: 16.4 us -> none  [the longest x2 5.7 us: update(): jnp.einsum('qhd,khd->hqk', queries[:, :, lower_col:lower_col + key_width]...]
    all_to_all x1 -> x0, waiting for transfers between devices: 12.2 us -> none  [sent_and_summed(): lax.all_to_all(parts, axis, split_axis=0, concat_axis=0, tiled=True)]
    all_to_all x1 -> x0, starting transfers between devices: 8.84 us -> none  [sent_and_summed(): lax.all_to_all(parts, axis, split_axis=0, concat_axis=0, tiled=True)]
    reduce_sum x6 -> x0, other arithmetic: 3.7 us -> none  [the longest x2 2.24 us: update(): new_tot.append(totals[member] * rescale + jnp.sum(weights, axis=-1))]
  transfers between devices with their start and end apart: 3 -> 0, of which waited for: 3 -> 0; matrix products, arithmetic and copies ran while one was open for 15% -> 0% of each run, Pallas kernels for 0% -> 0%
where the time goes in v1:
time: 129 us; the launch traced here: 128 us
  Pallas kernels  122 us (95%)
  local copies, waits for them, and re-layouts  5.43 us (4%)
    pallas_call x1, Pallas kernels, local(): pl.pallas_call(layer, out_shape=jax.ShapeDtypeStruct((SHARE, MODEL), bf),...  122 us

profile of v1, /device:TPU:1, one launch (start us, length us, event | category | flops | bytes accessed | tf_op | source)
XLA Modules:
  0.0 128.4 jit_solution(8892692242587861797)
XLA Ops:
  0.0 0.0 slice-start
  0.0 0.8 slice-done
  0.8 0.1 stack_reshape.6
  0.8 0.0 slice-start.2
  0.9 0.8 slice-done.2
  1.6 0.1 stack_reshape.7
  1.7 0.1 copy.14
  1.8 0.0 copy-start
  1.9 0.0 slice-start.3
  1.9 0.0 slice-start.1
  1.9 0.7 copy-done
  2.6 0.0 slice-done.3
  2.6 0.0 slice-done.1
  2.6 0.0 copy-start.1
  2.6 0.7 concatenate.16.shard_hbm
  3.4 0.0 copy-done.1
  3.4 0.6 reshape.27.mgain_ref
  4.6 122.2 %shard_map.109 = bf16[20,2048]{1,0:T(8,128)(2,1)} custom-call(f32[1]{0:T(128)S(6)} %copy.16.lam_ref, bf16[160,2048]{1,0:T(8,128)(2,1)} %resid_hbm.1, bf16[160,128]{1,0:T(8,128)(2,1)} %bitcast.12, bf16[160,128]{1,0:T(8,128)(2,1)} %bitcast.13, bf16[160,128]{1,0:T(8,128)(2,1)} %bitcast.14, bf16[1,128]{1,0:T(2,128)(2,1)} %bitcast.15, bf16[128,2048]{1,0:T(8,128)(2,1)} %wo_hbm.1, ...), custom_call_target="tpu_custom_call" | custom-call | tf_op jit(solution)/shard_map/pallas_call | solution.py:361
  126.9 1.5 %copy.17 = bf16[20,2048]{1,0:T(8,128)(2,1)} copy(bf16[20,2048]{1,0:T(8,128)(2,1)} %shard_map.109) | data formatting | bytes 163840
  (3 shorter events, 0.1 us)
Async XLA Ops:
  0.0 0.8 slice-start
  0.8 0.8 slice-start.2
  1.8 0.8 copy-start
  1.9 0.7 slice-start.3
  1.9 0.7 slice-start.1
  2.6 0.7 copy-start.1

commit v2 on v1

v2 whole, which is shorter than its diff:
```python
import functools

import jax
import jax.numpy as jnp
from jax import lax
from jax.experimental import pallas as pl
from jax.experimental.pallas import tpu as pltpu
from jax.sharding import PartitionSpec as P

MESH = pl.DeviceIdType.MESH
RING = 8
ROWS = 160
SHARE = 20
WIDTH = 128
MODEL = 2048
MAIN = 1280
REST = 896
OFFSETS = (0, 1, -1, 2, -2, 3, -3, 4)
FAR = -1e30
DIRS = (1, -1)
HALF_STEPS = {1: 4, -1: 3}


def hops(offset, d):
    return 4 if (d > 0) == (offset % 2 == 0) else 3


def onward(event):
    kind, d, k = event[0], event[-2], event[-1]
    if kind == "q" or kind == "kv":
        return [(kind, d, k + 1)] if k < HALF_STEPS[d] else []
    if kind == "r1":
        h = event[1]
        more = [("r1", h, d, k + 1)] if k < HALF_STEPS[d] else []
        return more + [("r2", h, d * k, e, 1) for e in DIRS]
    if kind == "r2":
        h, offset = event[1], event[2]
        return [("r2", h, offset, d, k + 1)] if k < hops(offset, d) else []
    return []


def plan():
    rate, latency = 46600.0, 1.9
    sizes = {"q": ROWS * WIDTH * 2, "kv": ROWS * WIDTH * 4}
    wide = (32 * MAIN * 2, 32 * REST * 2)
    free, arrivals, actions = {}, {}, []
    now = 0.0

    def send(event):
        kind, d = event[0], event[-2]
        if kind in sizes:
            size, axis = sizes[kind], kind == "kv"
        else:
            size, axis = wide[event[1]], (event[1] == 1) == (kind == "r1")
        done = max(free.get((axis, d), 0.0), now) + size / rate
        free[(axis, d)] = done
        arrivals[event] = done + latency

    for event in first_sends():
        send(event)
    ready = {"attend": None, "merge": None, "project": None}
    attended, read_at = 0, None
    while arrivals or ready["project"] != "done":
        if ready["attend"] is None and not any(e[0] in sizes for e in arrivals):
            ready["attend"] = now
        block = None
        if ready["attend"] is not None and attended < SEGMENTS:
            block = ("attend", attended, now, 2.5)
        elif attended == SEGMENTS and ready["merge"] != "done":
            block = ("merge", 0, read_at, 2.2)
        elif ready["merge"] == "done" and ready["project"] != "done":
            block = ("project", 0, read_at, 2.7)
        event = min(arrivals, key=lambda e: arrivals[e]) if arrivals else None
        if event is not None and (block is None or arrivals[event] <= max(now, block[2])):
            now = max(now, arrivals.pop(event))
            actions.append(event)
            for more in onward(event):
                send(more)
            continue
        now = max(now, block[2]) + block[3]
        actions.append(block[:2])
        if block[0] == "attend":
            for d in DIRS:
                free[(False, d)] = max(free.get((False, d), 0.0), now) + 8 * ROWS * WIDTH * 4 / rate / SEGMENTS
            attended += 1
            read_at = max(free[(False, d)] for d in DIRS) + 3.0
        else:
            ready[block[0]] = "done"
            read_at = now + 6.0
    return actions, now


def first_sends():
    first = [("kv", d, 1) for d in DIRS] + [("q", d, 1) for d in DIRS]
    first += [("r1", h, d, 1) for h in (1, 0) for d in DIRS]
    return first + [("r2", h, 0, d, 1) for h in (0, 1) for d in DIRS]


SEGMENTS = 4


def wrap(v):
    return lax.rem(v + 2 * RING, RING)


def nt_dot(a, b, precision=None):
    return lax.dot_general(
        a, b, (((1,), (1,)), ((), ())), preferred_element_type=jnp.float32, precision=precision
    )


def layer(
    lam_ref, resid_hbm, q_ref, k_ref, v_ref, hgain_ref, wo_hbm, mgain_ref, gate_ref, up_ref, down_ref, out_ref,
    wa, wb, wo_all, qg, kvg, vext, o_part, o_recv, st_part, st_recv, heads_out, heads_all,
    resid, mid, normed, hidden, piece, own_mid, d_send, d_recv,
    r1_ss, r1_rs, r2_ss, r2_rs, q_ss, q_rs, kv_ss, kv_rs,
    o_ss, o_rs, st_ss, st_rs, wo_ss, wo_rs, core_ss, core_rs, h_ss, h_rs, d_ss, d_rs, local_sem,
):
    sp = lax.axis_index("sp")
    tp = lax.axis_index("tp")
    z = lax.div(sp, RING)
    y = lax.rem(sp, RING)

    def at_zy(zz, yy):
        return {"sp": zz * RING + yy}

    def remote(src, dst, ss, rs, device):
        return pltpu.make_async_remote_copy(
            src_ref=src, dst_ref=dst, send_sem=ss, recv_sem=rs, device_id=device, device_id_type=MESH
        )

    barrier = pltpu.get_barrier_semaphore()
    for d in DIRS:
        pl.semaphore_signal(barrier, inc=1, device_id=at_zy(wrap(z + d), y), device_id_type=MESH)
    for j in range(1, RING):
        pl.semaphore_signal(barrier, inc=1, device_id=at_zy(z, wrap(y + j)), device_id_type=MESH)
        pl.semaphore_signal(barrier, inc=1, device_id={"tp": wrap(tp + j)}, device_id_type=MESH)

    local_resid = pltpu.make_async_copy(resid_hbm, resid, local_sem.at[0])
    local_wo = pltpu.make_async_copy(wo_hbm, wo_all.at[tp], local_sem.at[1])
    local_resid.start()
    local_wo.start()
    qg[y] = q_ref[...]
    kvg[z, 0] = k_ref[...]
    kvg[z, 1] = v_ref[...]
    for c in range(5):
        wa[z, y, :, 256 * c : 256 * c + WIDTH] = gate_ref[:, WIDTH * c : WIDTH * (c + 1)]
        wa[z, y, :, 256 * c + WIDTH : 256 * (c + 1)] = up_ref[:, WIDTH * c : WIDTH * (c + 1)]
    wb[z, y, :, 0:WIDTH] = jnp.concatenate([gate_ref[:, 640:], up_ref[:, 640:]], axis=1)
    wb[z, y, :, WIDTH : 6 * WIDTH] = down_ref[:, :640]
    wb[z, y, :, 6 * WIDTH :] = jnp.concatenate([down_ref[:, 640:], jnp.zeros((32, 64), jnp.bfloat16)], axis=1)
    pl.semaphore_wait(barrier, 2 + 2 * (RING - 1))

    def copy_of(event, arriving=False):
        kind, d, k = event[0], event[-2], event[-1]
        back = k if arriving else k - 1
        if kind == "q":
            slot = qg.at[wrap(y - d * back)]
            index = (d < 0) * 4 + k - 1
            return remote(slot, slot, q_ss.at[index], q_rs.at[index], at_zy(z, wrap(y + d)))
        if kind == "kv":
            slot = kvg.at[wrap(z - d * back)]
            index = (d < 0) * 4 + k - 1
            return remote(slot, slot, kv_ss.at[index], kv_rs.at[index], at_zy(wrap(z + d), y))
        h = event[1]
        buffer = wb if h else wa
        if kind == "r1":
            dz, dy = (d, 0) if h else (0, d)
            slot = buffer.at[wrap(z - dz * back), wrap(y - dy * back)]
            index = (h * 2 + (d < 0)) * 4 + k - 1
            return remote(slot, slot, r1_ss.at[index], r1_rs.at[index], at_zy(wrap(z + dz), wrap(y + dy)))
        offset = event[2]
        if h:
            slot = buffer.at[wrap(z - offset), wrap(y - d * back)]
            device = at_zy(z, wrap(y + d))
        else:
            slot = buffer.at[wrap(z - d * back), wrap(y - offset)]
            device = at_zy(wrap(z + d), y)
        index = ((h * 2 + (d < 0)) * RING + OFFSETS.index(offset)) * 4 + k - 1
        return remote(slot, slot, r2_ss.at[index], r2_rs.at[index], device)

    started = []

    def start(event):
        started.append(event)
        copy_of(event).start()

    for event in first_sends():
        start(event)

    def wo_copy(j, slot):
        return remote(wo_hbm, wo_all.at[slot], wo_ss.at[j], wo_rs.at[j], {"tp": wrap(tp + 2 * (j + 1))})

    partner = tp + 1 - 2 * lax.rem(tp, 2)

    def core_copy(j, slot):
        return remote(wo_all.at[slot], wo_all.at[slot], core_ss.at[j], core_rs.at[j], {"tp": partner})

    for j in (0, 2, 1):
        wo_copy(j, tp).start()
    vext[:, WIDTH:] = jnp.ones((RING * ROWS, WIDTH), jnp.bfloat16)

    lane = lax.broadcasted_iota(jnp.int32, (ROWS, WIDTH), 1)
    key_lane = lax.broadcasted_iota(jnp.int32, (1, RING * ROWS), 1)
    key_pos = key_lane + y * ROWS
    for j in range(1, RING):
        key_pos = key_pos + jnp.where(key_lane >= j * ROWS, (RING - 1) * ROWS, 0)
    row_iota = lax.broadcasted_iota(jnp.int32, (ROWS, 1), 0)
    pick = (
        lax.broadcasted_iota(jnp.int32, (8, WIDTH), 1) == 64 * lax.broadcasted_iota(jnp.int32, (8, WIDTH), 0)
    ).astype(jnp.float32)
    spread = (
        lax.div(lax.broadcasted_iota(jnp.int32, (8, 2 * WIDTH), 1), WIDTH)
        == lax.broadcasted_iota(jnp.int32, (8, 2 * WIDTH), 0)
    ).astype(jnp.float32)

    def far(i):
        return 4 + (i // 2 if i % 2 == 0 else -(i + 1) // 2) if isinstance(i, int) else 4 + jnp.where(
            lax.rem(i, 2) == 0, lax.div(i, 2), -lax.div(i + 1, 2))

    def o_copies(i):
        device = at_zy(z, wrap(y + far(i)))
        return (
            remote(o_part.at[i], o_recv.at[i], o_ss.at[i], o_rs.at[i], device),
            remote(st_part.at[i], st_recv.at[i], st_ss.at[i], st_rs.at[i], device),
        )

    def attend(i, carry):
        yq = wrap(y + far(i))
        q = qg[yq] * jnp.bfloat16(0.125)
        q_pos = z * (RING * ROWS) + yq * ROWS + row_iota
        seen = key_pos <= q_pos
        keys = kvg[:, 0].reshape(RING * ROWS, WIDTH)
        logs = []
        for m in range(2):
            half = (lane < 64) if m == 0 else (lane >= 64)
            qm = jnp.where(half, q.astype(jnp.float32), 0.0).astype(jnp.bfloat16)
            s = jnp.where(seen, nt_dot(qm, keys), FAR)
            top = jnp.max(s, axis=1, keepdims=True)
            p = jnp.exp(s - top).astype(jnp.bfloat16)
            both = jnp.dot(p, vext[...], preferred_element_type=jnp.float32)
            total = both[:, WIDTH:]
            o_part[i, m] = (both[:, :WIDTH] / total).astype(jnp.bfloat16)
            logs.append(top + jnp.log(total))
        st_part[i] = nt_dot(pick, jnp.where(lane < 64, logs[0], logs[1]), lax.Precision.HIGHEST)

        @pl.when(i < RING - 1)
        def _():
            for c in o_copies(i):
                c.start()

        return carry

    def attend_segment(n):
        if n == 0:
            vext[:, :WIDTH] = kvg[:, 1].reshape(RING * ROWS, WIDTH)
        per = RING // SEGMENTS
        lax.fori_loop(n * per, (n + 1) * per, attend, 0)
        if n == SEGMENTS - 1:
            local_wo.wait()
            for j in range(3):
                wo_copy(j, wrap(tp - 2 * (j + 1))).wait_recv()
            for j in range(4):
                core_copy(j, wrap(tp + 2 * j)).start()

    def h_copy(j, slot):
        lanes = pl.ds(pl.multiple_of(slot * WIDTH, WIDTH), WIDTH)
        return remote(heads_out, heads_all.at[:, lanes], h_ss.at[j], h_rs.at[j], {"tp": wrap(tp + j + 1)})

    def merge_heads():
        for i in range(RING - 1):
            for c in o_copies(i):
                c.wait_recv()
        parts = [o_recv.at[i] for i in range(RING - 1)] + [o_part.at[RING - 1]]
        stats = [st_recv[i] for i in range(RING - 1)] + [st_part[RING - 1]]
        stat = [lax.dot_general(st, spread, (((0,), (0,)), ((), ())), preferred_element_type=jnp.float32,
                                precision=lax.Precision.HIGHEST) for st in stats]
        readings = []
        for m in range(2):
            ls = [st[:, m * WIDTH : (m + 1) * WIDTH] for st in stat]
            top = functools.reduce(jnp.maximum, ls)
            share = [jnp.exp(l - top) for l in ls]
            total = functools.reduce(jnp.add, share)
            acc = functools.reduce(jnp.add, [w * o[m].astype(jnp.float32) for w, o in zip(share, parts)])
            readings.append(acc / total)
        diff = readings[0] - lam_ref[0] * readings[1]
        scale = lax.rsqrt(jnp.mean(diff * diff, axis=1, keepdims=True) + 1e-06)
        heads = (diff * scale * hgain_ref[...].astype(jnp.float32)).astype(jnp.bfloat16)
        heads_out[...] = heads
        for j in (2, 3, 4, 1, 5, 0, 6):
            h_copy(j, tp).start()
        heads_all[:, pl.ds(pl.multiple_of(tp * WIDTH, WIDTH), WIDTH)] = heads
        local_resid.wait()

    def project_rows():
        for j in range(4):
            core_copy(j, wrap(partner + 2 * j)).wait_recv()
        for j in range(7):
            h_copy(j, wrap(tp - j - 1)).wait_recv()

        def project(c, squares):
            lanes = pl.ds(pl.multiple_of(c * 256, 256), 256)
            w = wo_all[:, :, lanes].reshape(RING * WIDTH, 256)
            part = jnp.dot(heads_all[...], w, preferred_element_type=jnp.float32)
            m = (resid[:, lanes].astype(jnp.float32) + part).astype(jnp.bfloat16).astype(jnp.float32)
            mid[:, lanes] = m
            return squares + m[:, :WIDTH] * m[:, :WIDTH] + m[:, WIDTH:] * m[:, WIDTH:]

        squares = lax.fori_loop(0, 8, project, jnp.zeros((ROWS, WIDTH), jnp.float32))
        scale = lax.rsqrt(jnp.sum(squares, axis=1, keepdims=True) * (1.0 / MODEL) + 1e-06)

        def norm(c, carry):
            lanes = pl.ds(pl.multiple_of(c * 256, 256), 256)
            normed[:, lanes] = (mid[:, lanes] * scale * mgain_ref[:, lanes].astype(jnp.float32)).astype(jnp.bfloat16)
            return carry

        lax.fori_loop(0, 8, norm, 0)
        for t in range(RING):
            @pl.when(tp == t)
            def _():
                own_mid[...] = mid[t * SHARE : (t + 1) * SHARE, :]

    for action in plan()[0]:
        if action[0] == "attend":
            attend_segment(action[1])
        elif action[0] == "merge":
            merge_heads()
        elif action[0] == "project":
            project_rows()
        else:
            copy_of(action, True).wait_recv()
            for event in onward(action):
                start(event)

    def silu_times(g, u):
        return (g / (1.0 + jnp.exp(-g)) * u).astype(jnp.bfloat16)

    def gate_up(c, carry):
        w = wa[:, :, :, pl.ds(pl.multiple_of(c * 256, 256), 256)].reshape(MODEL, 256)
        r = jnp.dot(normed[...], w, preferred_element_type=jnp.float32)
        hidden[:, pl.ds(pl.multiple_of(c * WIDTH, WIDTH), WIDTH)] = silu_times(r[:, :WIDTH], r[:, WIDTH:])
        return carry

    lax.fori_loop(0, 5, gate_up, 0)
    r = jnp.dot(normed[...], wb[:, :, :, 0:WIDTH].reshape(MODEL, WIDTH), preferred_element_type=jnp.float32)
    r = jnp.where(lane < 64, silu_times(r, pltpu.roll(r, 64, 1)).astype(jnp.float32), 0.0)
    hidden[:, 5 * WIDTH :] = r.astype(jnp.bfloat16)

    def d_copy(j, part, dst_slot):
        lanes = pl.ds(part * (MODEL // 2), MODEL // 2)
        peer = wrap(tp + j + 1)
        index = part * 7 + j
        return remote(d_send.at[peer, :, lanes], d_recv.at[dst_slot, :, lanes], d_ss.at[index], d_rs.at[index],
                      {"tp": peer})

    def down(c, carry):
        w = wb[c, :, :, WIDTH:].reshape(256, REST - WIDTH)
        lanes = pl.ds(pl.multiple_of(c * 256, 256), 256)
        piece[...] = nt_dot(hidden[...], w)
        for t in range(RING):
            d_send[t, :, lanes] = piece[t * SHARE : (t + 1) * SHARE, :].astype(jnp.bfloat16)
        return carry

    for part in range(2):
        lax.fori_loop(4 * part, 4 * part + 4, down, 0)
        for j in (2, 3, 4, 1, 5, 0, 6):
            d_copy(j, part, tp).start()

    d_recv[tp] = d_send[tp]
    for part in range(2):
        for j in range(7):
            d_copy(j, part, wrap(tp - j - 1)).wait_recv()
    total = functools.reduce(jnp.add, [d_recv[t].astype(jnp.float32) for t in range(RING)])
    out_ref[...] = (own_mid[...] + 0.5 * total).astype(jnp.bfloat16)

    for event in started:
        copy_of(event).wait_send()
    for j in range(7):
        for c in o_copies(j):
            c.wait_send()
        h_copy(j, tp).wait_send()
        for part in range(2):
            d_copy(j, part, tp).wait_send()
    for j in range(3):
        wo_copy(j, tp).wait_send()
    for j in range(4):
        core_copy(j, wrap(tp + 2 * j)).wait_send()


def local(residual, queries, key_vectors, value_vecs, lambda_head, head_gain, w_out, mlp_gain, w_gate, w_up, w_down):
    vmem = pl.BlockSpec(memory_space=pltpu.VMEM)
    hbm = pl.BlockSpec(memory_space=pl.ANY)
    dma = pltpu.SemaphoreType.DMA
    bf, f32 = jnp.bfloat16, jnp.float32
    return pl.pallas_call(
        layer,
        out_shape=jax.ShapeDtypeStruct((SHARE, MODEL), bf),
        in_specs=[pl.BlockSpec(memory_space=pltpu.SMEM), hbm, vmem, vmem, vmem, vmem, hbm, vmem, vmem, vmem, vmem],
        out_specs=vmem,
        scratch_shapes=[
            pltpu.VMEM((RING, RING, 32, MAIN), bf),
            pltpu.VMEM((RING, RING, 32, REST), bf),
            pltpu.VMEM((RING, WIDTH, MODEL), bf),
            pltpu.VMEM((RING, ROWS, WIDTH), bf),
            pltpu.VMEM((RING, 2, ROWS, WIDTH), bf),
            pltpu.VMEM((RING * ROWS, 2 * WIDTH), bf),
            pltpu.VMEM((RING, 2, ROWS, WIDTH), bf),
            pltpu.VMEM((RING - 1, 2, ROWS, WIDTH), bf),
            pltpu.VMEM((RING, 8, ROWS), f32),
            pltpu.VMEM((RING - 1, 8, ROWS), f32),
            pltpu.VMEM((ROWS, WIDTH), bf),
            pltpu.VMEM((ROWS, RING * WIDTH), bf),
            pltpu.VMEM((ROWS, MODEL), bf),
            pltpu.VMEM((ROWS, MODEL), f32),
            pltpu.VMEM((ROWS, MODEL), bf),
            pltpu.VMEM((ROWS, REST - WIDTH), bf),
            pltpu.VMEM((ROWS, 256), f32),
            pltpu.VMEM((SHARE, MODEL), f32),
            pltpu.VMEM((RING, SHARE, MODEL), bf),
            pltpu.VMEM((RING, SHARE, MODEL), bf),
            dma((16,)), dma((16,)), dma((128,)), dma((128,)), dma((8,)), dma((8,)), dma((8,)), dma((8,)),
            dma((7,)), dma((7,)), dma((7,)), dma((7,)),
            dma((3,)), dma((3,)), dma((4,)), dma((4,)), dma((7,)), dma((7,)), dma((14,)), dma((14,)), dma((2,)),
        ],
        compiler_params=pltpu.CompilerParams(
            collective_id=0, has_side_effects=True, vmem_limit_bytes=56 * 1024 * 1024
        ),
    )(
        lambda_head, residual, queries.reshape(ROWS, WIDTH), key_vectors.reshape(ROWS, WIDTH),
        value_vecs.reshape(ROWS, WIDTH), head_gain.reshape(1, WIDTH), w_out, mlp_gain.reshape(1, MODEL),
        w_gate, w_up, w_down.T,
    )


def solution(mesh):
    in_specs = (
        P("sp", None), P("sp", "tp", None), P("sp", "tp", None), P("sp", "tp", None), P("tp"), P(),
        P("tp", None), P(), P("sp", "tp"), P("sp", "tp"), P("tp", "sp"),
    )
    return jax.shard_map(
        local, mesh=mesh, in_specs=in_specs, out_specs=P(("sp", "tp"), None), check_vma=False
    )
```

time: 129 us -> 108 us (0.84)
  Pallas kernels: 122 us -> 104 us
  local copies, waits for them, and re-layouts: 5.43 us -> 2.82 us
    pallas_call x1, Pallas kernels: 122 us -> 104 us  [local(): pl.pallas_call(layer, out_shape=jax.ShapeDtypeStruct((SHARE, MODEL), bf),...]
    slice x8 -> x0, local copies, waits for them, and re-layouts: 1.57 us -> none  [the longest x2 0.78 us: local(): w_gate[:, :640].reshape(depth, 5, WIDTH)]
where the time goes in v2:
time: 108 us; the launch traced here: 107 us
  Pallas kernels  104 us (96%)
  local copies, waits for them, and re-layouts  2.82 us (3%)
    pallas_call x1, Pallas kernels, local(): pl.pallas_call(layer, out_shape=jax.ShapeDtypeStruct((SHARE, MODEL), bf),...  104 us
    unnamed x3, local copies, waits for them, and re-layouts  2.22 us

profile of v2, /device:TPU:1, one launch (start us, length us, event | category | flops | bytes accessed | tf_op | source)
XLA Modules:
  0.0 107.5 jit_solution(4211757242193556679)
XLA Ops:
  0.7 0.0 copy-start
  0.7 0.7 copy-done
  1.3 0.6 reshape.19.mgain_ref
  1.9 104.0 %shard_map.109 = bf16[20,2048]{1,0:T(8,128)(2,1)} custom-call(f32[1]{0:T(128)S(6)} %copy.13.lam_ref, bf16[160,2048]{1,0:T(8,128)(2,1)} %resid_hbm.1, bf16[160,128]{1,0:T(8,128)(2,1)} %bitcast.6, bf16[160,128]{1,0:T(8,128)(2,1)} %bitcast.7, bf16[160,128]{1,0:T(8,128)(2,1)} %bitcast.8, bf16[1,128]{1,0:T(2,128)(2,1)} %bitcast.9, bf16[128,2048]{1,0:T(8,128)(2,1)} %wo_hbm.1, ...), custom_call_target="tpu_custom_call" | custom-call | tf_op jit(solution)/shard_map/pallas_call | solution.py:395
  105.9 1.5 %copy.14 = bf16[20,2048]{1,0:T(8,128)(2,1)} copy(bf16[20,2048]{1,0:T(8,128)(2,1)} %shard_map.109) | data formatting | bytes 163840
Async XLA Ops:
  0.7 0.7 copy-start

commit v3 on v2

--- a/solution.py
+++ b/solution.py
@@ -13,12 +13,14 @@
 SHARE = 20
 WIDTH = 128
 MODEL = 2048
-MAIN = 1280
-REST = 896
-OFFSETS = (0, 1, -1, 2, -2, 3, -3, 4)
 FAR = -1e30
 DIRS = (1, -1)
-HALF_STEPS = {1: 4, -1: 3}
+STEPS = {1: 4, -1: 3}
+SPREAD = {1: 3, -1: 4}
+OFFSETS = (0, 1, -1, 2, -2, 3, -3, -4)
+SEGMENTS = 8
+LIMIT = 3.25
+PIECES = ((0, 768), (1, 640), (0, 512), (1, 256))
 
 
 def hops(offset, d):
@@ -27,76 +29,112 @@
 
 def onward(event):
     kind, d, k = event[0], event[-2], event[-1]
-    if kind == "q" or kind == "kv":
-        return [(kind, d, k + 1)] if k < HALF_STEPS[d] else []
+    if kind in ("q", "kv"):
+        return [(kind, d, k + 1)] if k < STEPS[d] else []
     if kind == "r1":
-        h = event[1]
-        more = [("r1", h, d, k + 1)] if k < HALF_STEPS[d] else []
-        return more + [("r2", h, d * k, e, 1) for e in DIRS]
-    if kind == "r2":
-        h, offset = event[1], event[2]
-        return [("r2", h, offset, d, k + 1)] if k < hops(offset, d) else []
-    return []
-
-
-def plan():
+        more = [("r1", event[1], d, k + 1)] if k < SPREAD[d] else []
+        return more + [("r2", event[1], d * k, e, 1) for e in DIRS]
+    return [event[:-1] + (k + 1,)] if k < hops(event[2], d) else []
+
+
+def over_z(event):
+    if event[0] in ("q", "kv"):
+        return event[0] == "kv"
+    return (PIECES[event[1]][0] == 1) == (event[0] == "r1")
+
+
+def column_of(event):
+    if event[0] not in ("r1", "r2") or event[1] < 2:
+        return None
+    travel = event[-2] * event[-1]
+    along_z = travel if over_z(event) else (event[2] if event[0] == "r2" else 0)
+    return along_z % RING
+
+
+def plan(limit):
     rate, latency = 46600.0, 1.9
-    sizes = {"q": ROWS * WIDTH * 2, "kv": ROWS * WIDTH * 4}
-    wide = (32 * MAIN * 2, 32 * REST * 2)
-    free, arrivals, actions = {}, {}, []
+    free, arrivals, actions, held = {}, {}, [], []
     now = 0.0
-
-    def send(event):
-        kind, d = event[0], event[-2]
-        if kind in sizes:
-            size, axis = sizes[kind], kind == "kv"
+    missing = {r: (14 if r == 0 else 16) for r in range(RING)}
+    gated = 2 * (RING * RING - 1)
+
+    def rank(event):
+        return 0 if event[0] in ("q", "kv") else 1 + 2 * (event[1] // 2) + (event[0] == "r2")
+
+    def size(event):
+        if event[0] in ("q", "kv"):
+            return ROWS * WIDTH * (2 if event[0] == "q" else 4)
+        return 64 * PIECES[event[1]][1]
+
+    def release():
+        for event in sorted(held, key=rank):
+            link = (over_z(event), event[-2])
+            if rank(event) == 0 or free.get(link, 0.0) - now <= limit:
+                held.remove(event)
+                free[link] = max(free.get(link, 0.0), now) + size(event) / rate
+                arrivals[event] = free[link] + latency
+                actions.append(("start", event))
+
+    for d in DIRS:
+        held += [("kv", d, 1), ("q", d, 1)]
+    for p in range(4):
+        held += [("r1", p, d, 1) for d in DIRS] + [("r2", p, 0, d, 1) for d in DIRS]
+    release()
+    attended, stage, at = 0, "attend", None
+    rows = []
+    while arrivals or held or stage != "end":
+        if stage == "attend" and at is None and not any(e[0] in ("q", "kv") for e in list(arrivals) + held):
+            at = now
+        ready = None
+        if stage == "gate_up":
+            ready = now if gated == 0 else None
+        elif stage == "down":
+            ready = now if any(missing[r] == 0 and r not in rows for r in range(RING)) else None
+        elif stage != "end":
+            ready = at
+        event = min(arrivals, key=lambda e: arrivals[e]) if arrivals else None
+        if event is not None and (ready is None or arrivals[event] <= max(now, ready)):
+            now = max(now, arrivals.pop(event))
+            actions.append(("wait", event))
+            held += onward(event)
+            if column_of(event) is not None:
+                missing[column_of(event)] -= 1
+            elif event[0] in ("r1", "r2"):
+                gated -= 1
+        elif ready is None:
+            now += 0.3
         else:
-            size, axis = wide[event[1]], (event[1] == 1) == (kind == "r1")
-        done = max(free.get((axis, d), 0.0), now) + size / rate
-        free[(axis, d)] = done
-        arrivals[event] = done + latency
-
-    for event in first_sends():
-        send(event)
-    ready = {"attend": None, "merge": None, "project": None}
-    attended, read_at = 0, None
-    while arrivals or ready["project"] != "done":
-        if ready["attend"] is None and not any(e[0] in sizes for e in arrivals):
-            ready["attend"] = now
-        block = None
-        if ready["attend"] is not None and attended < SEGMENTS:
-            block = ("attend", attended, now, 2.5)
-        elif attended == SEGMENTS and ready["merge"] != "done":
-            block = ("merge", 0, read_at, 2.2)
-        elif ready["merge"] == "done" and ready["project"] != "done":
-            block = ("project", 0, read_at, 2.7)
-        event = min(arrivals, key=lambda e: arrivals[e]) if arrivals else None
-        if event is not None and (block is None or arrivals[event] <= max(now, block[2])):
-            now = max(now, arrivals.pop(event))
-            actions.append(event)
-            for more in onward(event):
-                send(more)
-            continue
-        now = max(now, block[2]) + block[3]
-        actions.append(block[:2])
-        if block[0] == "attend":
-            for d in DIRS:
-                free[(False, d)] = max(free.get((False, d), 0.0), now) + 8 * ROWS * WIDTH * 4 / rate / SEGMENTS
-            attended += 1
-            read_at = max(free[(False, d)] for d in DIRS) + 3.0
-        else:
-            ready[block[0]] = "done"
-            read_at = now + 6.0
+            now = max(now, ready)
+            if stage == "attend":
+                now += 1.3
+                actions.append(("attend", attended))
+                attended += 1
+                for d in DIRS:
+                    link = (False, d)
+                    free[link] = max(free.get(link, 0.0), now) + ROWS * WIDTH * 4 * RING / SEGMENTS / rate
+                if attended == SEGMENTS:
+                    stage, at = "merge", max(free[(False, d)] for d in DIRS) + 3.0
+            elif stage == "merge":
+                now += 2.0
+                actions.append(("merge", 0))
+                stage, at = "project", now + 5.0
+            elif stage == "project":
+                now += 2.6
+                actions.append(("project", 0))
+                stage = "gate_up"
+            elif stage == "gate_up":
+                now += 2.3
+                actions.append(("gate_up", 0))
+                stage = "down"
+            else:
+                row = [r for r in range(RING) if missing[r] == 0 and r not in rows][0]
+                now += 0.4
+                actions.append(("down", row))
+                rows.append(row)
+                if len(rows) == RING:
+                    stage = "end"
+        release()
     return actions, now
-
-
-def first_sends():
-    first = [("kv", d, 1) for d in DIRS] + [("q", d, 1) for d in DIRS]
-    first += [("r1", h, d, 1) for h in (1, 0) for d in DIRS]
-    return first + [("r2", h, 0, d, 1) for h in (0, 1) for d in DIRS]
-
-
-SEGMENTS = 4
 
 
 def wrap(v):
@@ -111,7 +149,7 @@
 
 def layer(
     lam_ref, resid_hbm, q_ref, k_ref, v_ref, hgain_ref, wo_hbm, mgain_ref, gate_ref, up_ref, down_ref, out_ref,
-    wa, wb, wo_all, qg, kvg, vext, o_part, o_recv, st_part, st_recv, heads_out, heads_all,
+    w0, w1, w2, w3, wo_all, qg, kvg, vext, o_part, o_recv, st_part, st_recv, heads_out, heads_all,
     resid, mid, normed, hidden, piece, own_mid, d_send, d_recv,
     r1_ss, r1_rs, r2_ss, r2_rs, q_ss, q_rs, kv_ss, kv_rs,
     o_ss, o_rs, st_ss, st_rs, wo_ss, wo_rs, core_ss, core_rs, h_ss, h_rs, d_ss, d_rs, local_sem,
@@ -144,11 +182,13 @@
     kvg[z, 0] = k_ref[...]
     kvg[z, 1] = v_ref[...]
     for c in range(5):
-        wa[z, y, :, 256 * c : 256 * c + WIDTH] = gate_ref[:, WIDTH * c : WIDTH * (c + 1)]
-        wa[z, y, :, 256 * c + WIDTH : 256 * (c + 1)] = up_ref[:, WIDTH * c : WIDTH * (c + 1)]
-    wb[z, y, :, 0:WIDTH] = jnp.concatenate([gate_ref[:, 640:], up_ref[:, 640:]], axis=1)
-    wb[z, y, :, WIDTH : 6 * WIDTH] = down_ref[:, :640]
-    wb[z, y, :, 6 * WIDTH :] = jnp.concatenate([down_ref[:, 640:], jnp.zeros((32, 64), jnp.bfloat16)], axis=1)
+        pair = w0.at[z, y, :, pl.ds(256 * c, 256)] if c < 3 else w1.at[z, y, :, pl.ds(256 * (c - 3), 256)]
+        pair[:, 0:WIDTH] = gate_ref[:, WIDTH * c : WIDTH * (c + 1)]
+        pair[:, WIDTH:] = up_ref[:, WIDTH * c : WIDTH * (c + 1)]
+    w1[z, y, :, 512:] = jnp.concatenate([gate_ref[:, 640:], up_ref[:, 640:]], axis=1)
+    w2[z, y] = down_ref[:, :512]
+    w3[z, y, :, :WIDTH] = down_ref[:, 512:640]
+    w3[z, y, :, WIDTH:] = jnp.concatenate([down_ref[:, 640:], jnp.zeros((32, 64), jnp.bfloat16)], axis=1)
     pl.semaphore_wait(barrier, 2 + 2 * (RING - 1))
 
     def copy_of(event, arriving=False):
@@ -162,21 +202,22 @@
             slot = kvg.at[wrap(z - d * back)]
             index = (d < 0) * 4 + k - 1
             return remote(slot, slot, kv_ss.at[index], kv_rs.at[index], at_zy(wrap(z + d), y))
-        h = event[1]
-        buffer = wb if h else wa
+        p = event[1]
+        buffer = (w0, w1, w2, w3)[p]
+        first_z = PIECES[p][0]
         if kind == "r1":
-            dz, dy = (d, 0) if h else (0, d)
+            dz, dy = (d, 0) if first_z else (0, d)
             slot = buffer.at[wrap(z - dz * back), wrap(y - dy * back)]
-            index = (h * 2 + (d < 0)) * 4 + k - 1
+            index = (p * 2 + (d < 0)) * 4 + k - 1
             return remote(slot, slot, r1_ss.at[index], r1_rs.at[index], at_zy(wrap(z + dz), wrap(y + dy)))
         offset = event[2]
-        if h:
+        if first_z:
             slot = buffer.at[wrap(z - offset), wrap(y - d * back)]
             device = at_zy(z, wrap(y + d))
         else:
             slot = buffer.at[wrap(z - d * back), wrap(y - offset)]
             device = at_zy(wrap(z + d), y)
-        index = ((h * 2 + (d < 0)) * RING + OFFSETS.index(offset)) * 4 + k - 1
+        index = ((p * 2 + (d < 0)) * RING + OFFSETS.index(offset)) * 4 + k - 1
         return remote(slot, slot, r2_ss.at[index], r2_rs.at[index], device)
 
     started = []
@@ -184,9 +225,6 @@
     def start(event):
         started.append(event)
         copy_of(event).start()
-
-    for event in first_sends():
-        start(event)
 
     def wo_copy(j, slot):
         return remote(wo_hbm, wo_all.at[slot], wo_ss.at[j], wo_rs.at[j], {"tp": wrap(tp + 2 * (j + 1))})
@@ -320,57 +358,63 @@
             def _():
                 own_mid[...] = mid[t * SHARE : (t + 1) * SHARE, :]
 
-    for action in plan()[0]:
-        if action[0] == "attend":
-            attend_segment(action[1])
-        elif action[0] == "merge":
-            merge_heads()
-        elif action[0] == "project":
-            project_rows()
-        else:
-            copy_of(action, True).wait_recv()
-            for event in onward(action):
-                start(event)
-
     def silu_times(g, u):
         return (g / (1.0 + jnp.exp(-g)) * u).astype(jnp.bfloat16)
 
-    def gate_up(c, carry):
-        w = wa[:, :, :, pl.ds(pl.multiple_of(c * 256, 256), 256)].reshape(MODEL, 256)
-        r = jnp.dot(normed[...], w, preferred_element_type=jnp.float32)
-        hidden[:, pl.ds(pl.multiple_of(c * WIDTH, WIDTH), WIDTH)] = silu_times(r[:, :WIDTH], r[:, WIDTH:])
-        return carry
-
-    lax.fori_loop(0, 5, gate_up, 0)
-    r = jnp.dot(normed[...], wb[:, :, :, 0:WIDTH].reshape(MODEL, WIDTH), preferred_element_type=jnp.float32)
-    r = jnp.where(lane < 64, silu_times(r, pltpu.roll(r, 64, 1)).astype(jnp.float32), 0.0)
-    hidden[:, 5 * WIDTH :] = r.astype(jnp.bfloat16)
-
-    def d_copy(j, part, dst_slot):
-        lanes = pl.ds(part * (MODEL // 2), MODEL // 2)
+    def gated_rows():
+        for buffer, first, pairs in ((w0, 0, 3), (w1, 3, 2)):
+            def gate_up(c, carry):
+                w = buffer[:, :, :, pl.ds(pl.multiple_of(c * 256, 256), 256)].reshape(MODEL, 256)
+                r = jnp.dot(normed[...], w, preferred_element_type=jnp.float32)
+                lanes = pl.ds(pl.multiple_of((c + first) * WIDTH, WIDTH), WIDTH)
+                hidden[:, lanes] = silu_times(r[:, :WIDTH], r[:, WIDTH:])
+                return carry
+
+            lax.fori_loop(0, pairs, gate_up, 0)
+        r = jnp.dot(normed[...], w1[:, :, :, 512:].reshape(MODEL, WIDTH), preferred_element_type=jnp.float32)
+        r = jnp.where(lane < 64, silu_times(r, pltpu.roll(r, 64, 1)).astype(jnp.float32), 0.0)
+        hidden[:, 5 * WIDTH :] = r.astype(jnp.bfloat16)
+
+    def d_copy(j, turn, row):
+        lanes = pl.ds(pl.multiple_of(wrap(z - row) * 256, 256), 256)
         peer = wrap(tp + j + 1)
-        index = part * 7 + j
-        return remote(d_send.at[peer, :, lanes], d_recv.at[dst_slot, :, lanes], d_ss.at[index], d_rs.at[index],
-                      {"tp": peer})
-
-    def down(c, carry):
-        w = wb[c, :, :, WIDTH:].reshape(256, REST - WIDTH)
-        lanes = pl.ds(pl.multiple_of(c * 256, 256), 256)
-        piece[...] = nt_dot(hidden[...], w)
+        index = turn * 7 + j
+        return remote(d_send.at[peer, :, lanes], d_recv.at[j, :, lanes], d_ss.at[index], d_rs.at[index], {"tp": peer})
+
+    def down_row(turn, row):
+        slot = wrap(z - row)
+        lanes = pl.ds(pl.multiple_of(slot * 256, 256), 256)
+        piece[...] = nt_dot(hidden[:, 0:512], w2[slot].reshape(256, 512)) + nt_dot(
+            hidden[:, 512:], w3[slot].reshape(256, 256)
+        )
         for t in range(RING):
             d_send[t, :, lanes] = piece[t * SHARE : (t + 1) * SHARE, :].astype(jnp.bfloat16)
-        return carry
-
-    for part in range(2):
-        lax.fori_loop(4 * part, 4 * part + 4, down, 0)
         for j in (2, 3, 4, 1, 5, 0, 6):
-            d_copy(j, part, tp).start()
-
-    d_recv[tp] = d_send[tp]
-    for part in range(2):
+            d_copy(j, turn, row).start()
+
+    turns = []
+    for kind, what in plan(LIMIT)[0]:
+        if kind == "attend":
+            attend_segment(what)
+        elif kind == "merge":
+            merge_heads()
+        elif kind == "project":
+            project_rows()
+        elif kind == "gate_up":
+            gated_rows()
+        elif kind == "down":
+            down_row(len(turns), what)
+            turns.append(what)
+        elif kind == "wait":
+            copy_of(what, True).wait_recv()
+        else:
+            start(what)
+
+    for turn, row in enumerate(turns):
         for j in range(7):
-            d_copy(j, part, wrap(tp - j - 1)).wait_recv()
-    total = functools.reduce(jnp.add, [d_recv[t].astype(jnp.float32) for t in range(RING)])
+            d_copy(j, turn, row).wait_recv()
+    total = functools.reduce(jnp.add, [d_recv[j].astype(jnp.float32) for j in range(RING - 1)])
+    total = total + d_send[tp].astype(jnp.float32)
     out_ref[...] = (own_mid[...] + 0.5 * total).astype(jnp.bfloat16)
 
     for event in started:
@@ -379,8 +423,8 @@
         for c in o_copies(j):
             c.wait_send()
         h_copy(j, tp).wait_send()
-        for part in range(2):
-            d_copy(j, part, tp).wait_send()
+        for turn, row in enumerate(turns):
+            d_copy(j, turn, row).wait_send()
     for j in range(3):
         wo_copy(j, tp).wait_send()
     for j in range(4):
@@ -398,8 +442,7 @@
         in_specs=[pl.BlockSpec(memory_space=pltpu.SMEM), hbm, vmem, vmem, vmem, vmem, hbm, vmem, vmem, vmem, vmem],
         out_specs=vmem,
         scratch_shapes=[
-            pltpu.VMEM((RING, RING, 32, MAIN), bf),
-            pltpu.VMEM((RING, RING, 32, REST), bf),
+            *[pltpu.VMEM((RING, RING, 32, lanes), bf) for _, lanes in PIECES],
             pltpu.VMEM((RING, WIDTH, MODEL), bf),
             pltpu.VMEM((RING, ROWS, WIDTH), bf),
             pltpu.VMEM((RING, 2, ROWS, WIDTH), bf),
@@ -413,14 +456,14 @@
             pltpu.VMEM((ROWS, MODEL), bf),
             pltpu.VMEM((ROWS, MODEL), f32),
             pltpu.VMEM((ROWS, MODEL), bf),
-            pltpu.VMEM((ROWS, REST - WIDTH), bf),
+            pltpu.VMEM((ROWS, 6 * WIDTH), bf),
             pltpu.VMEM((ROWS, 256), f32),
             pltpu.VMEM((SHARE, MODEL), f32),
             pltpu.VMEM((RING, SHARE, MODEL), bf),
-            pltpu.VMEM((RING, SHARE, MODEL), bf),
-            dma((16,)), dma((16,)), dma((128,)), dma((128,)), dma((8,)), dma((8,)), dma((8,)), dma((8,)),
+            pltpu.VMEM((RING - 1, SHARE, MODEL), bf),
+            dma((32,)), dma((32,)), dma((256,)), dma((256,)), dma((8,)), dma((8,)), dma((8,)), dma((8,)),
             dma((7,)), dma((7,)), dma((7,)), dma((7,)),
-            dma((3,)), dma((3,)), dma((4,)), dma((4,)), dma((7,)), dma((7,)), dma((14,)), dma((14,)), dma((2,)),
+            dma((3,)), dma((3,)), dma((4,)), dma((4,)), dma((7,)), dma((7,)), dma((56,)), dma((56,)), dma((2,)),
         ],
         compiler_params=pltpu.CompilerParams(
             collective_id=0, has_side_effects=True, vmem_limit_bytes=56 * 1024 * 1024

time: 108 us -> 102 us (0.944)
  Pallas kernels: 104 us -> 98.4 us
    pallas_call x1, Pallas kernels: 104 us -> 98.4 us  [local(): pl.pallas_call(layer, out_shape=jax.ShapeDtypeStruct((SHARE, MODEL), bf),...]
where the time goes in v3:
time: 102 us
  Pallas kernels  98.4 us (96%)
  local copies, waits for them, and re-layouts  2.82 us (3%)
    pallas_call x1, Pallas kernels, local(): pl.pallas_call(layer, out_shape=jax.ShapeDtypeStruct((SHARE, MODEL), bf),...  98.4 us
    unnamed x3, local copies, waits for them, and re-layouts  2.22 us

profile of v3, /device:TPU:1, one launch (start us, length us, event | category | flops | bytes accessed | tf_op | source)
XLA Modules:
  0.0 101.9 jit_solution(401404689913293626)
XLA Ops:
  0.7 0.0 copy-start
  0.7 0.7 copy-done
  1.3 0.6 reshape.19.mgain_ref
  1.9 98.4 %shard_map.109 = bf16[20,2048]{1,0:T(8,128)(2,1)} custom-call(f32[1]{0:T(128)S(6)} %copy.13.lam_ref, bf16[160,2048]{1,0:T(8,128)(2,1)} %resid_hbm.1, bf16[160,128]{1,0:T(8,128)(2,1)} %bitcast.6, bf16[160,128]{1,0:T(8,128)(2,1)} %bitcast.7, bf16[160,128]{1,0:T(8,128)(2,1)} %bitcast.8, bf16[1,128]{1,0:T(2,128)(2,1)} %bitcast.9, bf16[128,2048]{1,0:T(8,128)(2,1)} %wo_hbm.1, ...), custom_call_target="tpu_custom_call" | custom-call | tf_op jit(solution)/shard_map/pallas_call | solution.py:439
  100.3 1.5 %copy.14 = bf16[20,2048]{1,0:T(8,128)(2,1)} copy(bf16[20,2048]{1,0:T(8,128)(2,1)} %shard_map.109) | data formatting | bytes 163840
Async XLA Ops:
  0.7 0.7 copy-start

commit v4 on v3

v4 whole, which is shorter than its diff:
```python
import functools
import itertools

import jax
import jax.numpy as jnp
from jax import lax
from jax.experimental import pallas as pl
from jax.experimental.pallas import tpu as pltpu
from jax.sharding import PartitionSpec as P

MESH = pl.DeviceIdType.MESH
RING = 8
ROWS = 160
SHARE = 20
WIDTH = 128
MODEL = 2048
FAR = -1e30
DIRS = (1, -1)
STEPS = {1: 4, -1: 3}
SPREAD = {1: 3, -1: 4}
OFFSETS = (0, 1, -1, 2, -2, 3, -3, -4)
TURNS = ((1, 1), (-1, 1), (1, 2), (-1, 2), (1, 3), (-1, 3), (1, 4), (0, 0))
LIMITS = (1.8, 1.8, 2.5, 2.0)
PAIRS, DOWN = 3, 3
PIECES = ((0, 256 * PAIRS), (1, 1408 - 256 * PAIRS), (0, 128 * DOWN), (1, 768 - 128 * DOWN))


def hops(offset, d):
    return 4 if (d > 0) == (offset % 2 == 0) else 3


def onward(event):
    kind, d, k = event[0], event[-2], event[-1]
    if kind == "o":
        return []
    if kind in ("q", "kv"):
        return [(kind, d, k + 1)] if k < STEPS[d] else []
    if kind == "r1":
        more = [("r1", event[1], d, k + 1)] if k < SPREAD[d] else []
        return more + [("r2", event[1], d * k, e, 1) for e in DIRS]
    return [event[:-1] + (k + 1,)] if k < hops(event[2], d) else []


def last_gate(event):
    return event[0] == "r2" and event[1] < 2 and event[-1] == hops(event[2], event[3])


def own_flags():
    events = [("r1", p, d, k) for p in range(4) for d in DIRS for k in range(1, SPREAD[d] + 1)]
    events += [
        ("r2", p, o, d, k) for p in range(4) for o in OFFSETS for d in DIRS for k in range(1, hops(o, d) + 1)
    ]
    return {e: i for i, e in enumerate(e for e in events if not last_gate(e))}


def over_z(event):
    if event[0] in ("q", "kv", "o"):
        return event[0] == "kv"
    return (PIECES[event[1]][0] == 1) == (event[0] == "r1")


def column_of(event):
    if event[0] not in ("r1", "r2") or event[1] < 2:
        return None
    travel = event[-2] * event[-1]
    along_z = travel if over_z(event) else (event[2] if event[0] == "r2" else 0)
    return along_z % RING


def plan(limits):
    rate, latency = 46600.0, 2.2
    free, arrivals, actions, held = {}, {}, [], []
    now = 0.0
    missing = {r: (14 if r == 0 else 16) for r in range(RING)}
    gated = 2 * (RING * RING - 1)

    def rank(event):
        return 0 if event[0] in ("q", "kv", "o") else 1 + 2 * (event[1] // 2) + (event[0] == "r2")

    def size(event):
        if event[0] in ("q", "kv", "o"):
            return ROWS * WIDTH * (2 if event[0] == "q" else 4)
        return 64 * PIECES[event[1]][1]

    def release():
        for event in sorted(held, key=rank):
            link = (over_z(event), event[-2])
            if stage == "attend" and at is not None and not link[0]:
                calm = limits[1]
            else:
                calm = limits[3] if rank(event) > 2 else limits[0] if at is None else limits[2]
            if rank(event) == 0 or free.get(link, 0.0) - now <= calm:
                held.remove(event)
                free[link] = max(free.get(link, 0.0), now) + size(event) / rate
                arrivals[event] = free[link] + latency
                actions.append(("start", event))

    for d in DIRS:
        held += [("kv", d, 1), ("q", d, 1)]
    for p in range(4):
        held += [("r1", p, d, 1) for d in DIRS] + [("r2", p, 0, d, 1) for d in DIRS]
    attended, passed, stage, at, sent = 0, 0, "attend", None, 0.0
    release()
    came, rows = set(), []
    while arrivals or held or stage != "end":
        if at is None and not any(e[0] in ("q", "kv") for e in list(arrivals) + held):
            at = now
        block = None
        if stage == "attend" and at is not None:
            d, k = TURNS[passed]
            needed = {("o", 1, 4), ("o", -1, 3)} if d == 0 else {("o", d, k - 1)} if k > 1 else set()
            if passed < attended and needed <= came:
                block = ("merge", 0, 1.2) if d == 0 else ("pass", passed, 0.4)
            elif attended < len(TURNS):
                block = ("attend", attended, 1.3)
        elif stage == "project":
            block = ("project", 0, 2.6)
        elif stage == "gate_up" and gated == 0:
            block = ("gate_up", 0, 2.3)
        elif stage == "down":
            done = [r for r in range(RING) if missing[r] == 0 and r not in rows]
            if len(done) > 1:
                block = ("down", (done[0], done[1]), 0.8)
        ready = None if block is None else max(now, at) if stage == "project" else now
        event = min(arrivals, key=lambda e: arrivals[e]) if arrivals else None
        if event is not None and (block is None or arrivals[event] <= ready):
            now = max(now, arrivals.pop(event))
            actions.append(("wait", event))
            came.add(event)
            held += onward(event)
            if column_of(event) is not None:
                missing[column_of(event)] -= 1
            elif event[0] in ("r1", "r2"):
                gated -= 1
        elif block is None:
            now += 0.3
        else:
            now = ready + block[2]
            actions.append(block[:2])
            if block[0] == "attend":
                attended += 1
            elif block[0] == "pass":
                held.append(("o",) + TURNS[passed])
                passed += 1
            elif block[0] == "merge":
                stage, at = "project", now + 5.0
            elif block[0] == "project":
                stage = "gate_up"
            elif block[0] == "gate_up":
                stage = "down"
            else:
                rows += block[1]
                sent = max(sent, now) + 0.9
                if len(rows) == RING:
                    stage = "end"
        release()
    return actions, max(now, sent + 4.0)


def wrap(v):
    return lax.rem(v + 2 * RING, RING)


def nt_dot(a, b, precision=None):
    return lax.dot_general(
        a, b, (((1,), (1,)), ((), ())), preferred_element_type=jnp.float32, precision=precision
    )


def layer(
    lam_ref, resid_hbm, q_ref, k_ref, v_ref, hgain_ref, wo_hbm, mgain_ref, gate_ref, up_ref, down_ref, out_ref,
    w0, w1, w2, w3, wo_all, qg, kvg, vext, own_read, own_log, o_part, o_recv, st_part, st_recv, heads_out, heads_all,
    resid, mid, normed, hidden, piece, own_mid, d_own, d_near, d_pair, d_recv,
    ring_ss, ring_rs, last_rs, q_rs, kv_rs, o_rs, st_rs, near_rs, sent, came, local_sem,
):
    sp = lax.axis_index("sp")
    tp = lax.axis_index("tp")
    z = lax.div(sp, RING)
    y = lax.rem(sp, RING)

    def at_zy(zz, yy):
        return {"sp": zz * RING + yy}

    def remote(src, dst, ss, rs, device):
        return pltpu.make_async_remote_copy(
            src_ref=src, dst_ref=dst, send_sem=ss, recv_sem=rs, device_id=device, device_id_type=MESH
        )

    barrier = pltpu.get_barrier_semaphore()
    for d in DIRS:
        pl.semaphore_signal(barrier, inc=1, device_id=at_zy(wrap(z + d), y), device_id_type=MESH)
    for j in range(1, RING):
        pl.semaphore_signal(barrier, inc=1, device_id=at_zy(z, wrap(y + j)), device_id_type=MESH)
        pl.semaphore_signal(barrier, inc=1, device_id={"tp": wrap(tp + j)}, device_id_type=MESH)

    local_resid = pltpu.make_async_copy(resid_hbm, resid, local_sem.at[0])
    local_wo = pltpu.make_async_copy(wo_hbm, wo_all.at[tp], local_sem.at[1])
    local_resid.start()
    local_wo.start()
    qg[y] = q_ref[...]
    kvg[z, 0] = k_ref[...]
    kvg[z, 1] = v_ref[...]
    for c in range(5):
        pair = w0.at[z, y, :, pl.ds(256 * c, 256)] if c < PAIRS else w1.at[z, y, :, pl.ds(256 * (c - PAIRS), 256)]
        pair[:, 0:WIDTH] = gate_ref[:, WIDTH * c : WIDTH * (c + 1)]
        pair[:, WIDTH:] = up_ref[:, WIDTH * c : WIDTH * (c + 1)]
    w1[z, y, :, 256 * (5 - PAIRS) :] = jnp.concatenate([gate_ref[:, 640:], up_ref[:, 640:]], axis=1)
    w2[z, y] = down_ref[:, : PIECES[2][1]]
    w3[z, y, :, : PIECES[3][1] - WIDTH] = down_ref[:, PIECES[2][1] : 640]
    w3[z, y, :, PIECES[3][1] - WIDTH :] = jnp.concatenate([down_ref[:, 640:], jnp.zeros((32, 64), jnp.bfloat16)], axis=1)
    pl.semaphore_wait(barrier, 2 + 2 * (RING - 1))

    flags = own_flags()

    def copy_of(event, arriving=False):
        kind, d, k = event[0], event[-2], event[-1]
        back = k if arriving else k - 1
        if kind == "q":
            slot = qg.at[wrap(y - d * back)]
            index = (d < 0) * 4 + k - 1
            return remote(slot, slot, sent.at[0], q_rs.at[index], at_zy(z, wrap(y + d)))
        if kind == "kv":
            slot = kvg.at[wrap(z - d * back)]
            index = (d < 0) * 4 + k - 1
            return remote(slot, slot, sent.at[1], kv_rs.at[index], at_zy(wrap(z + d), y))
        p = event[1]
        buffer = (w0, w1, w2, w3)[p]
        first_z = PIECES[p][0]
        if kind == "r1":
            dz, dy = (d, 0) if first_z else (0, d)
            slot = buffer.at[wrap(z - dz * back), wrap(y - dy * back)]
            return remote(slot, slot, ring_ss.at[p], ring_rs.at[flags[event]], at_zy(wrap(z + dz), wrap(y + dy)))
        offset = event[2]
        if first_z:
            slot = buffer.at[wrap(z - offset), wrap(y - d * back)]
            device = at_zy(z, wrap(y + d))
        else:
            slot = buffer.at[wrap(z - d * back), wrap(y - offset)]
            device = at_zy(wrap(z + d), y)
        arrived = last_rs.at[p] if last_gate(event) else ring_rs.at[flags[event]]
        return remote(slot, slot, ring_ss.at[4 + p], arrived, device)

    def all_of(ref, ss, rs):
        return remote(ref, ref, ss, rs, {"tp": wrap(tp + 1)})

    def wo_copy(j, slot):
        return remote(wo_hbm, wo_all.at[slot], sent.at[2], came.at[2], {"tp": wrap(tp + 2 * (j + 1))})

    partner = tp + 1 - 2 * lax.rem(tp, 2)

    def core_copy(j, slot):
        return remote(wo_all.at[slot], wo_all.at[slot], sent.at[3], came.at[3], {"tp": partner})

    for j in (0, 2, 1):
        wo_copy(j, tp).start()
    vext[:, WIDTH:] = jnp.ones((RING * ROWS, WIDTH), jnp.bfloat16)

    lane = lax.broadcasted_iota(jnp.int32, (ROWS, WIDTH), 1)
    key_lane = lax.broadcasted_iota(jnp.int32, (1, RING * ROWS), 1)
    key_pos = key_lane + y * ROWS
    for j in range(1, RING):
        key_pos = key_pos + jnp.where(key_lane >= j * ROWS, (RING - 1) * ROWS, 0)
    row_iota = lax.broadcasted_iota(jnp.int32, (ROWS, 1), 0)
    pick = (
        lax.broadcasted_iota(jnp.int32, (8, WIDTH), 1) == 64 * lax.broadcasted_iota(jnp.int32, (8, WIDTH), 0)
    ).astype(jnp.float32)
    spread = (
        lax.div(lax.broadcasted_iota(jnp.int32, (8, 2 * WIDTH), 1), WIDTH)
        == lax.broadcasted_iota(jnp.int32, (8, 2 * WIDTH), 0)
    ).astype(jnp.float32)

    def o_copies(i):
        device = at_zy(z, wrap(y + TURNS[i][0]))
        return (
            remote(o_part.at[i], o_recv.at[i], sent.at[4], o_rs.at[i], device),
            remote(st_part.at[i], st_recv.at[i], sent.at[5], st_rs.at[i], device),
        )

    def attend(i):
        if i == 0:
            vext[:, :WIDTH] = kvg[:, 1].reshape(RING * ROWS, WIDTH)
        d, k = TURNS[i]
        yq = wrap(y + (5 - k if d > 0 else k - 4 if d < 0 else 0))
        q = qg[yq] * jnp.bfloat16(0.125)
        q_pos = z * (RING * ROWS) + yq * ROWS + row_iota
        seen = key_pos <= q_pos
        keys = kvg[:, 0].reshape(RING * ROWS, WIDTH)
        for m in range(2):
            half = (lane < 64) if m == 0 else (lane >= 64)
            qm = jnp.where(half, q.astype(jnp.float32), 0.0).astype(jnp.bfloat16)
            s = jnp.where(seen, nt_dot(qm, keys), FAR)
            top = jnp.max(s, axis=1, keepdims=True)
            p = jnp.exp(s - top).astype(jnp.bfloat16)
            both = jnp.dot(p, vext[...], preferred_element_type=jnp.float32)
            total = both[:, WIDTH:]
            own_read[i, m] = both[:, :WIDTH] / total
            own_log[i, m] = top + jnp.log(total)

    def merged(i, incoming):
        stats = [
            lax.dot_general(st_recv[n], spread, (((0,), (0,)), ((), ())), preferred_element_type=jnp.float32,
                            precision=lax.Precision.HIGHEST) for n in incoming
        ]
        out = []
        for m in range(2):
            logs = [own_log[i, m]] + [st[:, m * WIDTH : (m + 1) * WIDTH] for st in stats]
            reads = [own_read[i, m]] + [o_recv[n, m].astype(jnp.float32) for n in incoming]
            if not incoming:
                out.append((reads[0], logs[0]))
                continue
            top = functools.reduce(jnp.maximum, logs)
            share = [jnp.exp(l - top) for l in logs]
            total = functools.reduce(jnp.add, share)
            read = functools.reduce(jnp.add, [w * o for w, o in zip(share, reads)]) / total
            out.append((read, top + jnp.log(total)))
        return out

    def pass_on(i):
        d, k = TURNS[i]
        out = merged(i, [TURNS.index((d, k - 1))] if k > 1 else [])
        for m in range(2):
            o_part[i, m] = out[m][0].astype(jnp.bfloat16)
        st_part[i] = nt_dot(pick, jnp.where(lane < 64, out[0][1], out[1][1]), lax.Precision.HIGHEST)

    def share_projection():
        local_wo.wait()
        all_of(wo_all.at[pl.ds(0, 3)], sent.at[2], came.at[2]).wait_recv()
        for j in range(4):
            core_copy(j, wrap(tp + 2 * j)).start()

    def h_copy(j, slot):
        lanes = pl.ds(pl.multiple_of(slot * WIDTH, WIDTH), WIDTH)
        return remote(heads_out, heads_all.at[:, lanes], sent.at[6], came.at[6], {"tp": wrap(tp + j + 1)})

    def merge_heads():
        readings = [read for read, _ in merged(7, [TURNS.index((1, 4)), TURNS.index((-1, 3))])]
        diff = readings[0] - lam_ref[0] * readings[1]
        scale = lax.rsqrt(jnp.mean(diff * diff, axis=1, keepdims=True) + 1e-06)
        heads = (diff * scale * hgain_ref[...].astype(jnp.float32)).astype(jnp.bfloat16)
        heads_out[...] = heads
        for j in (2, 3, 4, 1, 5, 0, 6):
            h_copy(j, tp).start()
        heads_all[:, pl.ds(pl.multiple_of(tp * WIDTH, WIDTH), WIDTH)] = heads
        local_resid.wait()

    def project_rows():
        all_of(wo_all.at[pl.ds(0, 4)], sent.at[3], came.at[3]).wait_recv()
        all_of(heads_all.at[:, pl.ds(0, 7 * WIDTH)], sent.at[6], came.at[6]).wait_recv()

        def project(c, squares):
            lanes = pl.ds(pl.multiple_of(c * 256, 256), 256)
            w = wo_all[:, :, lanes].reshape(RING * WIDTH, 256)
            part = jnp.dot(heads_all[...], w, preferred_element_type=jnp.float32)
            m = (resid[:, lanes].astype(jnp.float32) + part).astype(jnp.bfloat16).astype(jnp.float32)
            mid[:, lanes] = m
            return squares + m[:, :WIDTH] * m[:, :WIDTH] + m[:, WIDTH:] * m[:, WIDTH:]

        squares = lax.fori_loop(0, 8, project, jnp.zeros((ROWS, WIDTH), jnp.float32))
        scale = lax.rsqrt(jnp.sum(squares, axis=1, keepdims=True) * (1.0 / MODEL) + 1e-06)

        def norm(c, carry):
            lanes = pl.ds(pl.multiple_of(c * 256, 256), 256)
            normed[:, lanes] = (mid[:, lanes] * scale * mgain_ref[:, lanes].astype(jnp.float32)).astype(jnp.bfloat16)
            return carry

        lax.fori_loop(0, 8, norm, 0)
        for t in range(RING):
            @pl.when(tp == t)
            def _():
                own_mid[...] = mid[t * SHARE : (t + 1) * SHARE, :]

    def silu_times(g, u):
        return (g / (1.0 + jnp.exp(-g)) * u).astype(jnp.bfloat16)

    def gated_rows():
        for p, buffer in ((0, w0), (1, w1)):
            all_of(buffer.at[pl.ds(0, 2)], ring_ss.at[4 + p], last_rs.at[p]).wait_recv()
        for buffer, first, pairs in ((w0, 0, PAIRS), (w1, PAIRS, 5 - PAIRS)):
            def gate_up(c, carry):
                w = buffer[:, :, :, pl.ds(pl.multiple_of(c * 256, 256), 256)].reshape(MODEL, 256)
                r = jnp.dot(normed[...], w, preferred_element_type=jnp.float32)
                lanes = pl.ds(pl.multiple_of((c + first) * WIDTH, WIDTH), WIDTH)
                hidden[:, lanes] = silu_times(r[:, :WIDTH], r[:, WIDTH:])
                return carry

            lax.fori_loop(0, pairs, gate_up, 0)
        r = jnp.dot(normed[...], w1[:, :, :, 256 * (5 - PAIRS) :].reshape(MODEL, WIDTH), preferred_element_type=jnp.float32)
        r = jnp.where(lane < 64, silu_times(r, pltpu.roll(r, 64, 1)).astype(jnp.float32), 0.0)
        hidden[:, 5 * WIDTH :] = r.astype(jnp.bfloat16)

    core = lax.rem(tp, 2)

    def lanes_of(row):
        return pl.ds(pl.multiple_of(wrap(z - row) * 256, 256), 256)

    def near_copy(turn, row):
        src = d_own.at[:, 1 - core, :, lanes_of(row)]
        return remote(src, d_near.at[:, :, lanes_of(row)], sent.at[8], near_rs.at[turn], {"tp": partner})

    def d_copy(j, row):
        peer = wrap(tp + 2 * (j + 1))
        src = d_pair.at[lax.div(peer, 2), :, lanes_of(row)]
        return remote(src, d_recv.at[j, :, lanes_of(row)], sent.at[7], came.at[7], {"tp": peer})

    def add_pair(turn, pair):
        for n, row in enumerate(pair):
            near_copy(2 * turn + n, row).wait_recv()
        for row, q in itertools.product(pair, range(RING // 2)):
            both = d_own[q, core, :, lanes_of(row)].astype(jnp.float32) + d_near[q, :, lanes_of(row)].astype(jnp.float32)
            d_pair[q, :, lanes_of(row)] = both.astype(jnp.bfloat16)
        for row, j in itertools.product(pair, (1, 0, 2)):
            d_copy(j, row).start()

    def down_pair(turn, pair):
        for n, row in enumerate(pair):
            slot = wrap(z - row)
            piece[n] = nt_dot(hidden[:, : PIECES[2][1]], w2[slot].reshape(256, PIECES[2][1])) + nt_dot(
                hidden[:, PIECES[2][1] :], w3[slot].reshape(256, PIECES[3][1])
            )
        for n, row in enumerate(pair):
            for t in range(RING):
                d_own[t // 2, t % 2, :, lanes_of(row)] = piece[n, t * SHARE : (t + 1) * SHARE, :].astype(jnp.bfloat16)
        for n, row in enumerate(pair):
            near_copy(2 * turn + n, row).start()

    turns = []
    for kind, what in plan(LIMITS)[0]:
        if kind == "attend":
            attend(what)
        elif kind == "pass":
            pass_on(what)
        elif kind == "merge":
            share_projection()
            merge_heads()
        elif kind == "project":
            project_rows()
        elif kind == "gate_up":
            gated_rows()
        elif kind == "down":
            down_pair(len(turns), what)
            if turns:
                add_pair(len(turns) - 1, turns[-1])
            turns.append(what)
        elif kind == "wait":
            if what[0] == "o":
                for c in o_copies(TURNS.index(what[1:])):
                    c.wait_recv()
            elif not last_gate(what):
                copy_of(what, True).wait_recv()
        elif what[0] == "o":
            for c in o_copies(TURNS.index(what[1:])):
                c.start()
        else:
            copy_of(what).start()

    add_pair(len(turns) - 1, turns[-1])
    all_of(d_recv, sent.at[7], came.at[7]).wait_recv()
    total = functools.reduce(jnp.add, [d_recv[j].astype(jnp.float32) for j in range(RING // 2 - 1)])
    total = total + d_pair[lax.div(tp, 2)].astype(jnp.float32)
    out_ref[...] = (own_mid[...] + 0.5 * total).astype(jnp.bfloat16)

    for ref, n in (
        (qg.at[pl.ds(0, 7)], 0), (kvg.at[pl.ds(0, 7)], 1), (wo_all.at[pl.ds(0, 3)], 2), (wo_all.at[pl.ds(0, 4)], 3),
        (o_recv, 4), (st_recv, 5), (heads_all.at[:, pl.ds(0, 7 * WIDTH)], 6), (d_recv, 7),
        (d_near, 8),
    ):
        all_of(ref, sent.at[n], came.at[0]).wait_send()
    for p, buffer in enumerate((w0, w1, w2, w3)):
        all_of(buffer.at[0, pl.ds(0, 7)], ring_ss.at[p], last_rs.at[0]).wait_send()
        all_of(buffer.at[pl.ds(0, 7)], ring_ss.at[4 + p], last_rs.at[0]).wait_send()


def local(residual, queries, key_vectors, value_vecs, lambda_head, head_gain, w_out, mlp_gain, w_gate, w_up, w_down):
    vmem = pl.BlockSpec(memory_space=pltpu.VMEM)
    hbm = pl.BlockSpec(memory_space=pl.ANY)
    dma = pltpu.SemaphoreType.DMA
    bf, f32 = jnp.bfloat16, jnp.float32
    return pl.pallas_call(
        layer,
        out_shape=jax.ShapeDtypeStruct((SHARE, MODEL), bf),
        in_specs=[pl.BlockSpec(memory_space=pltpu.SMEM), hbm, vmem, vmem, vmem, vmem, hbm, vmem, vmem, vmem, vmem],
        out_specs=vmem,
        scratch_shapes=[
            *[pltpu.VMEM((RING, RING, 32, lanes), bf) for _, lanes in PIECES],
            pltpu.VMEM((RING, WIDTH, MODEL), bf),
            pltpu.VMEM((RING, ROWS, WIDTH), bf),
            pltpu.VMEM((RING, 2, ROWS, WIDTH), bf),
            pltpu.VMEM((RING * ROWS, 2 * WIDTH), bf),
            pltpu.VMEM((RING, 2, ROWS, WIDTH), f32),
            pltpu.VMEM((RING, 2, ROWS, WIDTH), f32),
            pltpu.VMEM((RING - 1, 2, ROWS, WIDTH), bf),
            pltpu.VMEM((RING - 1, 2, ROWS, WIDTH), bf),
            pltpu.VMEM((RING - 1, 8, ROWS), f32),
            pltpu.VMEM((RING - 1, 8, ROWS), f32),
            pltpu.VMEM((ROWS, WIDTH), bf),
            pltpu.VMEM((ROWS, RING * WIDTH), bf),
            pltpu.VMEM((ROWS, MODEL), bf),
            pltpu.VMEM((ROWS, MODEL), f32),
            pltpu.VMEM((ROWS, MODEL), bf),
            pltpu.VMEM((ROWS, 6 * WIDTH), bf),
            pltpu.VMEM((2, ROWS, 256), f32),
            pltpu.VMEM((SHARE, MODEL), f32),
            pltpu.VMEM((RING // 2, 2, SHARE, MODEL), bf),
            pltpu.VMEM((RING // 2, SHARE, MODEL), bf),
            pltpu.VMEM((RING // 2, SHARE, MODEL), bf),
            pltpu.VMEM((RING // 2 - 1, SHARE, MODEL), bf),
            dma((8,)), dma((len(own_flags()),)), dma((2,)), dma((8,)), dma((8,)), dma((7,)), dma((7,)), dma((8,)), dma((9,)), dma((8,)), dma((2,)),
        ],
        compiler_params=pltpu.CompilerParams(
            collective_id=0, has_side_effects=True, vmem_limit_bytes=56 * 1024 * 1024
        ),
    )(
        lambda_head, residual, queries.reshape(ROWS, WIDTH), key_vectors.reshape(ROWS, WIDTH),
        value_vecs.reshape(ROWS, WIDTH), head_gain.reshape(1, WIDTH), w_out, mlp_gain.reshape(1, MODEL),
        w_gate, w_up, w_down.T,
    )


def solution(mesh):
    in_specs = (
        P("sp", None), P("sp", "tp", None), P("sp", "tp", None), P("sp", "tp", None), P("tp"), P(),
        P("tp", None), P(), P("sp", "tp"), P("sp", "tp"), P("tp", "sp"),
    )
    return jax.shard_map(
        local, mesh=mesh, in_specs=in_specs, out_specs=P(("sp", "tp"), None), check_vma=False
    )
```

time: 102 us -> 92.7 us (0.909)
  Pallas kernels: 98.4 us -> 88.9 us
    pallas_call x1, Pallas kernels: 98.4 us -> 88.9 us  [local(): pl.pallas_call(layer, out_shape=jax.ShapeDtypeStruct((SHARE, MODEL), bf),...]
where the time goes in v4:
time: 92.7 us; the launch traced here: 92.4 us
  Pallas kernels  88.9 us (96%)
  local copies, waits for them, and re-layouts  2.82 us (3%)
    pallas_call x1, Pallas kernels, local(): pl.pallas_call(layer, out_shape=jax.ShapeDtypeStruct((SHARE, MODEL), bf),...  88.9 us
    unnamed x3, local copies, waits for them, and re-layouts  2.22 us

profile of v4, /device:TPU:1, one launch (start us, length us, event | category | flops | bytes accessed | tf_op | source)
XLA Modules:
  0.0 92.4 jit_solution(4374395281391704248)
XLA Ops:
  0.7 0.0 copy-start
  0.7 0.7 copy-done
  1.3 0.6 reshape.19.mgain_ref
  1.9 88.9 %shard_map.109 = bf16[20,2048]{1,0:T(8,128)(2,1)} custom-call(f32[1]{0:T(128)S(6)} %copy.13.lam_ref, bf16[160,2048]{1,0:T(8,128)(2,1)} %resid_hbm.1, bf16[160,128]{1,0:T(8,128)(2,1)} %bitcast.6, bf16[160,128]{1,0:T(8,128)(2,1)} %bitcast.7, bf16[160,128]{1,0:T(8,128)(2,1)} %bitcast.8, bf16[1,128]{1,0:T(2,128)(2,1)} %bitcast.9, bf16[128,2048]{1,0:T(8,128)(2,1)} %wo_hbm.1, ...), custom_call_target="tpu_custom_call" | custom-call | tf_op jit(solution)/shard_map/pallas_call | solution.py:478
  90.9 1.5 %copy.14 = bf16[20,2048]{1,0:T(8,128)(2,1)} copy(bf16[20,2048]{1,0:T(8,128)(2,1)} %shard_map.109) | data formatting | bytes 163840
Async XLA Ops:
  0.7 0.7 copy-start

commit v5 on v4

--- a/solution.py
+++ b/solution.py
@@ -22,6 +22,8 @@
 TURNS = ((1, 1), (-1, 1), (1, 2), (-1, 2), (1, 3), (-1, 3), (1, 4), (0, 0))
 LIMITS = (1.8, 1.8, 2.5, 2.0)
 PAIRS, DOWN = 3, 3
+TAIL = 6
+DELAY = 2.2
 PIECES = ((0, 256 * PAIRS), (1, 1408 - 256 * PAIRS), (0, 128 * DOWN), (1, 768 - 128 * DOWN))
 
 
@@ -68,7 +70,7 @@
 
 
 def plan(limits):
-    rate, latency = 46600.0, 2.2
+    rate, latency = 46600.0, DELAY
     free, arrivals, actions, held = {}, {}, [], []
     now = 0.0
     missing = {r: (14 if r == 0 else 16) for r in range(RING)}
@@ -119,8 +121,9 @@
             block = ("gate_up", 0, 2.3)
         elif stage == "down":
             done = [r for r in range(RING) if missing[r] == 0 and r not in rows]
-            if len(done) > 1:
-                block = ("down", (done[0], done[1]), 0.8)
+            take = 2 if len(rows) < TAIL else 1
+            if len(done) >= take:
+                block = ("down", tuple(done[:take]), 0.4 * take)
         ready = None if block is None else max(now, at) if stage == "project" else now
         event = min(arrivals, key=lambda e: arrivals[e]) if arrivals else None
         if event is not None and (block is None or arrivals[event] <= ready):
@@ -150,7 +153,7 @@
                 stage = "down"
             else:
                 rows += block[1]
-                sent = max(sent, now) + 0.9
+                sent = max(sent, now) + 0.45 * len(block[1])
                 if len(rows) == RING:
                     stage = "end"
         release()
@@ -168,7 +171,8 @@
 
 
 def layer(
-    lam_ref, resid_hbm, q_ref, k_ref, v_ref, hgain_ref, wo_hbm, mgain_ref, gate_ref, up_ref, down_ref, out_ref,
+    lam_ref, resid_hbm, q_hbm, k_hbm, v_hbm, hgain_ref, wo_hbm, mgain_ref, gate_hbm, up_hbm, down_hbm, out_ref,
+    gate_ref, up_ref, down_ref,
     w0, w1, w2, w3, wo_all, qg, kvg, vext, own_read, own_log, o_part, o_recv, st_part, st_recv, heads_out, heads_all,
     resid, mid, normed, hidden, piece, own_mid, d_own, d_near, d_pair, d_recv,
     ring_ss, ring_rs, last_rs, q_rs, kv_rs, o_rs, st_rs, near_rs, sent, came, local_sem,
@@ -186,6 +190,16 @@
             src_ref=src, dst_ref=dst, send_sem=ss, recv_sem=rs, device_id=device, device_id_type=MESH
         )
 
+    local_copies = [
+        pltpu.make_async_copy(src, dst, local_sem.at[n])
+        for n, (src, dst) in enumerate((
+            (k_hbm, kvg.at[z, 0]), (v_hbm, kvg.at[z, 1]), (q_hbm, qg.at[y]), (gate_hbm, gate_ref), (up_hbm, up_ref),
+            (down_hbm, down_ref), (wo_hbm, wo_all.at[tp]), (resid_hbm, resid),
+        ))
+    ]
+    token_copies, weight_copies, (local_wo, local_resid) = local_copies[:3], local_copies[3:6], local_copies[6:]
+    for c in local_copies:
+        c.start()
     barrier = pltpu.get_barrier_semaphore()
     for d in DIRS:
         pl.semaphore_signal(barrier, inc=1, device_id=at_zy(wrap(z + d), y), device_id_type=MESH)
@@ -193,22 +207,23 @@
         pl.semaphore_signal(barrier, inc=1, device_id=at_zy(z, wrap(y + j)), device_id_type=MESH)
         pl.semaphore_signal(barrier, inc=1, device_id={"tp": wrap(tp + j)}, device_id_type=MESH)
 
-    local_resid = pltpu.make_async_copy(resid_hbm, resid, local_sem.at[0])
-    local_wo = pltpu.make_async_copy(wo_hbm, wo_all.at[tp], local_sem.at[1])
-    local_resid.start()
-    local_wo.start()
-    qg[y] = q_ref[...]
-    kvg[z, 0] = k_ref[...]
-    kvg[z, 1] = v_ref[...]
-    for c in range(5):
-        pair = w0.at[z, y, :, pl.ds(256 * c, 256)] if c < PAIRS else w1.at[z, y, :, pl.ds(256 * (c - PAIRS), 256)]
-        pair[:, 0:WIDTH] = gate_ref[:, WIDTH * c : WIDTH * (c + 1)]
-        pair[:, WIDTH:] = up_ref[:, WIDTH * c : WIDTH * (c + 1)]
-    w1[z, y, :, 256 * (5 - PAIRS) :] = jnp.concatenate([gate_ref[:, 640:], up_ref[:, 640:]], axis=1)
-    w2[z, y] = down_ref[:, : PIECES[2][1]]
-    w3[z, y, :, : PIECES[3][1] - WIDTH] = down_ref[:, PIECES[2][1] : 640]
-    w3[z, y, :, PIECES[3][1] - WIDTH :] = jnp.concatenate([down_ref[:, 640:], jnp.zeros((32, 64), jnp.bfloat16)], axis=1)
+    for c in token_copies:
+        c.wait()
     pl.semaphore_wait(barrier, 2 + 2 * (RING - 1))
+
+    def pack():
+        for c in weight_copies:
+            c.wait()
+        for c in range(5):
+            pair = w0.at[z, y, :, pl.ds(256 * c, 256)] if c < PAIRS else w1.at[z, y, :, pl.ds(256 * (c - PAIRS), 256)]
+            pair[:, 0:WIDTH] = gate_ref[:, WIDTH * c : WIDTH * (c + 1)]
+            pair[:, WIDTH:] = up_ref[:, WIDTH * c : WIDTH * (c + 1)]
+        w1[z, y, :, 256 * (5 - PAIRS) :] = jnp.concatenate([gate_ref[:, 640:], up_ref[:, 640:]], axis=1)
+        w2[z, y] = down_ref[:, : PIECES[2][1]]
+        w3[z, y, :, : PIECES[3][1] - WIDTH] = down_ref[:, PIECES[2][1] : 640]
+        w3[z, y, :, PIECES[3][1] - WIDTH :] = jnp.concatenate(
+            [down_ref[:, 640:], jnp.zeros((32, 64), jnp.bfloat16)], axis=1
+        )
 
     flags = own_flags()
 
@@ -251,8 +266,6 @@
     def core_copy(j, slot):
         return remote(wo_all.at[slot], wo_all.at[slot], sent.at[3], came.at[3], {"tp": partner})
 
-    for j in (0, 2, 1):
-        wo_copy(j, tp).start()
     vext[:, WIDTH:] = jnp.ones((RING * ROWS, WIDTH), jnp.bfloat16)
 
     lane = lax.broadcasted_iota(jnp.int32, (ROWS, WIDTH), 1)
@@ -358,12 +371,10 @@
         squares = lax.fori_loop(0, 8, project, jnp.zeros((ROWS, WIDTH), jnp.float32))
         scale = lax.rsqrt(jnp.sum(squares, axis=1, keepdims=True) * (1.0 / MODEL) + 1e-06)
 
-        def norm(c, carry):
-            lanes = pl.ds(pl.multiple_of(c * 256, 256), 256)
-            normed[:, lanes] = (mid[:, lanes] * scale * mgain_ref[:, lanes].astype(jnp.float32)).astype(jnp.bfloat16)
-            return carry
-
-        lax.fori_loop(0, 8, norm, 0)
+        gains = mgain_ref[...].astype(jnp.float32)
+        for c in range(MODEL // WIDTH):
+            lanes = pl.ds(c * WIDTH, WIDTH)
+            normed[:, lanes] = (mid[:, lanes] * scale * gains[c : c + 1]).astype(jnp.bfloat16)
         for t in range(RING):
             @pl.when(tp == t)
             def _():
@@ -404,7 +415,7 @@
 
     def add_pair(turn, pair):
         for n, row in enumerate(pair):
-            near_copy(2 * turn + n, row).wait_recv()
+            near_copy(turn + n, row).wait_recv()
         for row, q in itertools.product(pair, range(RING // 2)):
             both = d_own[q, core, :, lanes_of(row)].astype(jnp.float32) + d_near[q, :, lanes_of(row)].astype(jnp.float32)
             d_pair[q, :, lanes_of(row)] = both.astype(jnp.bfloat16)
@@ -421,9 +432,9 @@
             for t in range(RING):
                 d_own[t // 2, t % 2, :, lanes_of(row)] = piece[n, t * SHARE : (t + 1) * SHARE, :].astype(jnp.bfloat16)
         for n, row in enumerate(pair):
-            near_copy(2 * turn + n, row).start()
-
-    turns = []
+            near_copy(turn + n, row).start()
+
+    turns, packed = [], False
     for kind, what in plan(LIMITS)[0]:
         if kind == "attend":
             attend(what)
@@ -437,9 +448,9 @@
         elif kind == "gate_up":
             gated_rows()
         elif kind == "down":
-            down_pair(len(turns), what)
+            down_pair(sum(map(len, turns)), what)
             if turns:
-                add_pair(len(turns) - 1, turns[-1])
+                add_pair(sum(map(len, turns[:-1])), turns[-1])
             turns.append(what)
         elif kind == "wait":
             if what[0] == "o":
@@ -451,9 +462,14 @@
             for c in o_copies(TURNS.index(what[1:])):
                 c.start()
         else:
+            if what[0] in ("r1", "r2") and not packed:
+                pack()
+                for j in (0, 2, 1):
+                    wo_copy(j, tp).start()
+                packed = True
             copy_of(what).start()
 
-    add_pair(len(turns) - 1, turns[-1])
+    add_pair(RING - len(turns[-1]), turns[-1])
     all_of(d_recv, sent.at[7], came.at[7]).wait_recv()
     total = functools.reduce(jnp.add, [d_recv[j].astype(jnp.float32) for j in range(RING // 2 - 1)])
     total = total + d_pair[lax.div(tp, 2)].astype(jnp.float32)
@@ -478,9 +494,12 @@
     return pl.pallas_call(
         layer,
         out_shape=jax.ShapeDtypeStruct((SHARE, MODEL), bf),
-        in_specs=[pl.BlockSpec(memory_space=pltpu.SMEM), hbm, vmem, vmem, vmem, vmem, hbm, vmem, vmem, vmem, vmem],
+        in_specs=[pl.BlockSpec(memory_space=pltpu.SMEM), hbm, hbm, hbm, hbm, vmem, hbm, vmem, hbm, hbm, hbm],
         out_specs=vmem,
         scratch_shapes=[
+            pltpu.VMEM((32, 704), bf),
+            pltpu.VMEM((32, 704), bf),
+            pltpu.VMEM((32, 704), bf),
             *[pltpu.VMEM((RING, RING, 32, lanes), bf) for _, lanes in PIECES],
             pltpu.VMEM((RING, WIDTH, MODEL), bf),
             pltpu.VMEM((RING, ROWS, WIDTH), bf),
@@ -504,14 +523,14 @@
             pltpu.VMEM((RING // 2, SHARE, MODEL), bf),
             pltpu.VMEM((RING // 2, SHARE, MODEL), bf),
             pltpu.VMEM((RING // 2 - 1, SHARE, MODEL), bf),
-            dma((8,)), dma((len(own_flags()),)), dma((2,)), dma((8,)), dma((8,)), dma((7,)), dma((7,)), dma((8,)), dma((9,)), dma((8,)), dma((2,)),
+            dma((8,)), dma((len(own_flags()),)), dma((2,)), dma((8,)), dma((8,)), dma((7,)), dma((7,)), dma((8,)), dma((9,)), dma((8,)), dma((8,)),
         ],
         compiler_params=pltpu.CompilerParams(
             collective_id=0, has_side_effects=True, vmem_limit_bytes=56 * 1024 * 1024
         ),
     )(
         lambda_head, residual, queries.reshape(ROWS, WIDTH), key_vectors.reshape(ROWS, WIDTH),
-        value_vecs.reshape(ROWS, WIDTH), head_gain.reshape(1, WIDTH), w_out, mlp_gain.reshape(1, MODEL),
+        value_vecs.reshape(ROWS, WIDTH), head_gain.reshape(1, WIDTH), w_out, mlp_gain.reshape(MODEL // WIDTH, WIDTH),
         w_gate, w_up, w_down.T,
     )
 

time: 92.7 us -> 90.2 us (0.973)
  local copies, waits for them, and re-layouts: 2.82 us -> 1.54 us
  Pallas kernels: 88.9 us -> 87.8 us
    pallas_call x1, Pallas kernels: 88.9 us -> 87.8 us  [local(): pl.pallas_call(layer, out_shape=jax.ShapeDtypeStruct((SHARE, MODEL), bf),...]
    unnamed x3 -> x1, local copies, waits for them, and re-layouts: 2.22 us -> 1.54 us
where the time goes in v5:
time: 90.2 us; the launch traced here: 90 us
  Pallas kernels  87.8 us (97%)
  local copies, waits for them, and re-layouts  1.54 us (2%)
    pallas_call x1, Pallas kernels, local(): pl.pallas_call(layer, out_shape=jax.ShapeDtypeStruct((SHARE, MODEL), bf),...  87.8 us

profile of v5, /device:TPU:1, one launch (start us, length us, event | category | flops | bytes accessed | tf_op | source)
XLA Modules:
  0.0 90.0 jit_solution(3064028188156940314)
XLA Ops:
  0.7 87.8 %shard_map.109 = bf16[20,2048]{1,0:T(8,128)(2,1)} custom-call(f32[1]{0:T(128)S(6)} %copy.13.lam_ref, bf16[160,2048]{1,0:T(8,128)(2,1)} %resid_hbm.1, bf16[160,128]{1,0:T(8,128)(2,1)} %bitcast.7, bf16[160,128]{1,0:T(8,128)(2,1)} %bitcast.8, bf16[160,128]{1,0:T(8,128)(2,1)} %bitcast.9, bf16[1,128]{1,0:T(2,128)(2,1)} %bitcast.11, bf16[128,2048]{1,0:T(8,128)(2,1)} %wo_hbm.1, ...), custom_call_target="tpu_custom_call" | custom-call | tf_op jit(solution)/shard_map/pallas_call | solution.py:494
  88.4 1.5 %copy.14 = bf16[20,2048]{1,0:T(8,128)(2,1)} copy(bf16[20,2048]{1,0:T(8,128)(2,1)} %shard_map.109) | data formatting | bytes 163840

commit v6 on v5

--- a/solution.py
+++ b/solution.py
@@ -174,7 +174,7 @@
     lam_ref, resid_hbm, q_hbm, k_hbm, v_hbm, hgain_ref, wo_hbm, mgain_ref, gate_hbm, up_hbm, down_hbm, out_ref,
     gate_ref, up_ref, down_ref,
     w0, w1, w2, w3, wo_all, qg, kvg, vext, own_read, own_log, o_part, o_recv, st_part, st_recv, heads_out, heads_all,
-    resid, mid, normed, hidden, piece, own_mid, d_own, d_near, d_pair, d_recv,
+    resid, mid, normed, hidden, piece, own_mid, d_own, d_near, d_pair, d_recv, d_last,
     ring_ss, ring_rs, last_rs, q_rs, kv_rs, o_rs, st_rs, near_rs, sent, came, local_sem,
 ):
     sp = lax.axis_index("sp")
@@ -413,6 +413,11 @@
         src = d_pair.at[lax.div(peer, 2), :, lanes_of(row)]
         return remote(src, d_recv.at[j, :, lanes_of(row)], sent.at[7], came.at[7], {"tp": peer})
 
+    def last_copy(j, row):
+        peer = wrap(tp + j + 1)
+        src = d_own.at[lax.div(peer, 2), lax.rem(peer, 2), :, lanes_of(row)]
+        return remote(src, d_last.at[j], sent.at[9], came.at[1], {"tp": peer})
+
     def add_pair(turn, pair):
         for n, row in enumerate(pair):
             near_copy(turn + n, row).wait_recv()
@@ -432,7 +437,11 @@
             for t in range(RING):
                 d_own[t // 2, t % 2, :, lanes_of(row)] = piece[n, t * SHARE : (t + 1) * SHARE, :].astype(jnp.bfloat16)
         for n, row in enumerate(pair):
-            near_copy(turn + n, row).start()
+            if turn + n == RING - 1:
+                for j in (2, 3, 4, 1, 5, 0, 6):
+                    last_copy(j, row).start()
+            else:
+                near_copy(turn + n, row).start()
 
     turns, packed = [], False
     for kind, what in plan(LIMITS)[0]:
@@ -469,16 +478,20 @@
                 packed = True
             copy_of(what).start()
 
-    add_pair(RING - len(turns[-1]), turns[-1])
-    all_of(d_recv, sent.at[7], came.at[7]).wait_recv()
+    all_of(d_recv.at[:, :, pl.ds(0, 7 * 256)], sent.at[7], came.at[7]).wait_recv()
     total = functools.reduce(jnp.add, [d_recv[j].astype(jnp.float32) for j in range(RING // 2 - 1)])
     total = total + d_pair[lax.div(tp, 2)].astype(jnp.float32)
     out_ref[...] = (own_mid[...] + 0.5 * total).astype(jnp.bfloat16)
+    all_of(d_last, sent.at[9], came.at[1]).wait_recv()
+    lanes = lanes_of(turns[-1][-1])
+    total = d_own[lax.div(tp, 2), core, :, lanes].astype(jnp.float32)
+    total = functools.reduce(jnp.add, [d_last[j].astype(jnp.float32) for j in range(RING - 1)], total)
+    out_ref[:, lanes] = (own_mid[:, lanes] + 0.5 * total).astype(jnp.bfloat16)
 
     for ref, n in (
         (qg.at[pl.ds(0, 7)], 0), (kvg.at[pl.ds(0, 7)], 1), (wo_all.at[pl.ds(0, 3)], 2), (wo_all.at[pl.ds(0, 4)], 3),
-        (o_recv, 4), (st_recv, 5), (heads_all.at[:, pl.ds(0, 7 * WIDTH)], 6), (d_recv, 7),
-        (d_near, 8),
+        (o_recv, 4), (st_recv, 5), (heads_all.at[:, pl.ds(0, 7 * WIDTH)], 6), (d_recv.at[:, :, pl.ds(0, 7 * 256)], 7),
+        (d_near.at[:, :, pl.ds(0, 7 * 256)], 8), (d_last, 9),
     ):
         all_of(ref, sent.at[n], came.at[0]).wait_send()
     for p, buffer in enumerate((w0, w1, w2, w3)):
@@ -523,7 +536,8 @@
             pltpu.VMEM((RING // 2, SHARE, MODEL), bf),
             pltpu.VMEM((RING // 2, SHARE, MODEL), bf),
             pltpu.VMEM((RING // 2 - 1, SHARE, MODEL), bf),
-            dma((8,)), dma((len(own_flags()),)), dma((2,)), dma((8,)), dma((8,)), dma((7,)), dma((7,)), dma((8,)), dma((9,)), dma((8,)), dma((8,)),
+            pltpu.VMEM((RING - 1, SHARE, 256), bf),
+            dma((8,)), dma((len(own_flags()),)), dma((2,)), dma((8,)), dma((8,)), dma((7,)), dma((7,)), dma((8,)), dma((10,)), dma((8,)), dma((8,)),
         ],
         compiler_params=pltpu.CompilerParams(
             collective_id=0, has_side_effects=True, vmem_limit_bytes=56 * 1024 * 1024

time: 90.2 us -> 90 us (level)
  no operation moved by 1% of the time
where the time goes in v6:
time: 90 us; the launch traced here: 89.8 us
  Pallas kernels  87.6 us (97%)
  local copies, waits for them, and re-layouts  1.54 us (2%)
    pallas_call x1, Pallas kernels, local(): pl.pallas_call(layer, out_shape=jax.ShapeDtypeStruct((SHARE, MODEL), bf),...  87.6 us

profile of v6, /device:TPU:1, one launch (start us, length us, event | category | flops | bytes accessed | tf_op | source)
XLA Modules:
  0.0 89.8 jit_solution(11545030630818820769)
XLA Ops:
  0.7 87.6 %shard_map.109 = bf16[20,2048]{1,0:T(8,128)(2,1)} custom-call(f32[1]{0:T(128)S(6)} %copy.13.lam_ref, bf16[160,2048]{1,0:T(8,128)(2,1)} %resid_hbm.1, bf16[160,128]{1,0:T(8,128)(2,1)} %bitcast.7, bf16[160,128]{1,0:T(8,128)(2,1)} %bitcast.8, bf16[160,128]{1,0:T(8,128)(2,1)} %bitcast.9, bf16[1,128]{1,0:T(2,128)(2,1)} %bitcast.11, bf16[128,2048]{1,0:T(8,128)(2,1)} %wo_hbm.1, ...), custom_call_target="tpu_custom_call" | custom-call | tf_op jit(solution)/shard_map/pallas_call | solution.py:507
  88.2 1.5 %copy.14 = bf16[20,2048]{1,0:T(8,128)(2,1)} copy(bf16[20,2048]{1,0:T(8,128)(2,1)} %shard_map.109) | data formatting | bytes 163840
